TPU v7x, 1024 devices: a whole 4x8x16 slice. The times are simulated.
1024 devices in a mesh: sp: 256 (over z, y, core), tp: 4 (over x).
Axes of the slice: x: 4, y: 8, z: 16, core: 2. Of those that a mesh axis runs over, the one named last changes fastest.
Arguments:
- tokens: bfloat16 [196608, 2048], P(('sp', 'tp')), may hold values from -6 to 6
- norm_gain: float32 [2048], replicated, may hold values from 0.1 to 1.9
- query_weight: bfloat16 [2048, 512], P(None, 'tp'), may hold values from -4 to 4
- key_weight: bfloat16 [2048, 256], P(None, 'tp'), may hold values from -4 to 4
- value_weight: bfloat16 [2048, 256], P(None, 'tp'), may hold values from -1 to 1
- sink_logit: float32 [8], P('tp'), may hold values from 2 to 6
- conv_gate_weight: bfloat16 [2048, 512], P(None, 'tp'), may hold values from -0.125 to 0.125
- conv_pre_weight: bfloat16 [2048, 512], P(None, 'tp'), may hold values from -0.125 to 0.125
- conv_input_weight: bfloat16 [2048, 512], P(None, 'tp'), may hold values from -0.125 to 0.125
- conv_taps: float32 [3, 512], P(None, 'tp'), may hold values from -3.5 to 3.5
- out_weight: bfloat16 [1024, 2048], replicated, may hold values from -0.1875 to 0.1875
Outputs:
- mixed: bfloat16 [196608, 2048], P(('sp', 'tp'))
All inputs are finite; a program needn't handle non-finite values.
Results may differ from a plain program's by a relative error of at most 0.009.
Values may be sent and summed in bfloat16 or wider, within the bound.
No kernel may reach another device: no remote copies, remote signals or barrier semaphores. Data moves between devices by JAX's collectives and lax.ppermute only.
A program may use at most 32 MiB of HBM per device.

v0:
```python
import jax
import jax.numpy as jnp
from jax import lax
from jax.sharding import PartitionSpec as P

QH = 8
KVH = 4
HEAD_SIZE = 64
WIN = 128


def extended(block, sides, width):
    for axis, dim in sides:
        count = lax.axis_size(axis)
        forward = [(i, i + 1) for i in range(count - 1)]
        backward = [(target, source) for source, target in forward]
        low = lax.ppermute(
            lax.slice_in_dim(block, block.shape[dim] - width, None, axis=dim), axis, forward
        )
        high = lax.ppermute(lax.slice_in_dim(block, 0, width, axis=dim), axis, backward)
        block = jnp.concatenate([low, block, high], axis=dim)
    return block


def attend_local(query_block_tile, key_block_tile, value_block_tile, start, sinks, total):
    count = query_block_tile.shape[0]
    span = key_block_tile.shape[0]
    score_matrix = jnp.einsum(
        "yxpz,ixz->xpyi", query_block_tile, key_block_tile, preferred_element_type=jnp.float32
    ) * HEAD_SIZE ** (-0.5)
    query_pos = start + jnp.arange(count, dtype=jnp.int32)
    key_pos = start - WIN + jnp.arange(span, dtype=jnp.int32)
    valid = (
        (jnp.abs(query_pos[:, None] - key_pos[None, :]) <= WIN)
        & (key_pos[None, :] >= 0)
        & (key_pos[None, :] < total)
    )
    score_matrix = jnp.where(valid[None, None], score_matrix, -jnp.inf)
    sink_col = sinks[:, :, None, None]
    top = jnp.maximum(jnp.max(score_matrix, axis=-1, keepdims=True), sink_col)
    expo = jnp.exp(score_matrix - top)
    denom = jnp.sum(expo, axis=-1, keepdims=True) + jnp.exp(sink_col - top)
    weight_lower_precision = (expo / denom).astype(jnp.bfloat16)
    final_output = jnp.einsum(
        "bhcv,vbn->cbhn",
        weight_lower_precision,
        value_block_tile,
        preferred_element_type=jnp.float32,
    )
    return final_output.reshape(count, -1).astype(jnp.bfloat16)


def short_conv(conv_pad, conv_taps, conv_gate):
    count = conv_gate.shape[0]
    conv_f = conv_pad.astype(jnp.float32)
    convolved = (
        conv_taps[0] * conv_f[0:count]
        + conv_taps[1] * conv_f[1 : count + 1]
        + conv_taps[2] * conv_f[2 : count + 2]
    )
    return (conv_gate.astype(jnp.float32) * convolved).astype(jnp.bfloat16)


def body(
    tokens,
    norm_gain,
    query_weight,
    key_weight,
    value_weight,
    sink_logit,
    conv_gate_weight,
    conv_pre_weight,
    conv_input_weight,
    conv_taps,
    out_weight,
):
    tokens_f = tokens.astype(jnp.float32)
    normed = (
        tokens_f
        * lax.rsqrt(jnp.mean(tokens_f * tokens_f, axis=-1, keepdims=True) + 1e-06)
        * norm_gain
    ).astype(jnp.bfloat16)
    all_weight = jnp.concatenate(
        [
            query_weight,
            key_weight,
            value_weight,
            conv_gate_weight,
            conv_pre_weight,
            conv_input_weight,
        ],
        axis=1,
    )
    projected = jnp.dot(
        lax.all_gather(normed, "tp", axis=0, tiled=True),
        all_weight,
        preferred_element_type=jnp.float32,
    ).astype(jnp.bfloat16)
    query_width = query_weight.shape[1]
    kv_width = key_weight.shape[1]
    conv_width = conv_gate_weight.shape[1]
    edge_key = query_width + kv_width
    edge_value = edge_key + kv_width
    edge_gate = edge_value + conv_width
    edge_pre = edge_gate + conv_width
    queries = projected[:, :query_width]
    key_rows = projected[:, query_width:edge_key]
    value_rows = projected[:, edge_key:edge_value]
    conv_gate = projected[:, edge_value:edge_gate]
    conv_pre = projected[:, edge_gate:edge_pre]
    conv_input = projected[:, edge_pre:]
    product = (conv_pre.astype(jnp.float32) * conv_input.astype(jnp.float32)).astype(jnp.bfloat16)
    count = projected.shape[0]
    offset = lax.axis_index("sp") * count
    total = count * lax.axis_size("sp")
    padded = extended(jnp.concatenate([key_rows, value_rows, product], 1), (("sp", 0),), WIN)
    key_pad = padded[:, :kv_width]
    value_pad = padded[:, kv_width : 2 * kv_width]
    conv_pad = padded[WIN - 1 : WIN + count + 1, 2 * kv_width :]
    groups = kv_width // HEAD_SIZE
    ratio = QH // KVH
    query_block_tile = queries.reshape(count, groups, ratio, HEAD_SIZE)
    key_block_tile = key_pad.reshape(-1, groups, HEAD_SIZE)
    value_block_tile = value_pad.reshape(-1, groups, HEAD_SIZE)
    sinks = sink_logit.reshape(groups, ratio)
    conv_out = short_conv(conv_pad, conv_taps, conv_gate)
    attended = attend_local(
        query_block_tile, key_block_tile, value_block_tile, offset, sinks, total
    )
    attn_rows, conv_rows = (
        lax.all_to_all(attended, "tp", split_axis=0, concat_axis=1, tiled=True),
        lax.all_to_all(conv_out, "tp", split_axis=0, concat_axis=1, tiled=True),
    )
    joined = jnp.concatenate([attn_rows, conv_rows], axis=1)
    return jnp.dot(joined, out_weight, preferred_element_type=jnp.float32).astype(jnp.bfloat16)


def solution(mesh):
    placed = (
        P(("sp", "tp"), None),
        P(),
        P(None, "tp"),
        P(None, "tp"),
        P(None, "tp"),
        P("tp"),
        P(None, "tp"),
        P(None, "tp"),
        P(None, "tp"),
        P(None, "tp"),
        P(),
    )
    return jax.shard_map(
        body, mesh=mesh, in_specs=placed, out_specs=P(("sp", "tp"), None), check_vma=False
    )
```

profile of v0, /device:TPU:1, one launch (start us, length us, event | category | flops | bytes accessed | tf_op | source)
XLA Modules:
  0.0 114.0 jit_solution(7738797985582582212)
XLA Ops:
  6.5 0.0 all-gather.2.cloned.1.call-start
  6.5 1.4 %fusion.6 = f32[192]{0:T(256)S(1)} fusion(bf16[192,2048]{1,0:T(8,128)(2,1)} %param.11), kind=kLoop, calls=%fused_computation.13 | loop fusion | flops 1179456 | bytes 787200 | tf_op jit(solution)/shard_map/reduce_sum | solution.py:80
  7.9 2.3 %fusion.8 = bf16[192,2048]{1,0:T(8,128)(2,1)} fusion(bf16[192,2048]{1,0:T(8,128)(2,1)} %param.11, f32[2048]{0:T(1024)} %param.12, f32[192]{0:T(256)S(1)} %add_rsqrt_fusion), kind=kLoop, calls=%fused_computation.15 | loop fusion | flops 1572864 | bytes 1581824 | tf_op jit(solution)/shard_map/convert_element_type | solution.py:82
  10.2 0.0 all-gather.2.cloned.1.call-update
  10.2 1.2 %copy.21 = bf16[2048,64]{1,0:T(8,128)(2,1)S(1)} copy(bf16[2048,64]{0,1:T(8,128)(2,1)} %param.14) | data formatting | bytes 524288 | tf_op args[3]
  11.4 2.0 %copy.22 = bf16[2048,64]{1,0:T(8,128)(2,1)} copy(bf16[2048,64]{0,1:T(8,128)(2,1)} %param.15) | data formatting | bytes 524288 | tf_op args[4]
  13.4 4.6 %concatenate.13 = bf16[2048,640]{1,0:T(8,128)(2,1)S(1)} concatenate(bf16[2048,128]{1,0:T(8,128)(2,1)} %param.13, bf16[2048,64]{1,0:T(8,128)(2,1)S(1)} %copy.21, bf16[2048,64]{1,0:T(8,128)(2,1)} %copy.22, bf16[2048,128]{1,0:T(8,128)(2,1)} %param.17, bf16[2048,128]{1,0:T(8,128)(2,1)} %param.18, bf16[2048,128]{1,0:T(8,128)(2,1)} %param.19), dimensions={1} | concatenate | bytes 5242880 | tf_op jit(solution)/shard_map/concatenate | solution.py:83
  18.0 1.4 %fusion.5 = pred[768,1024]{0,1:T(8,128)(4,1)S(1)} fusion(s32[1024]{0:T(1024)S(1)} %iota_add_fusion, s32[768]{0:T(1024)S(1)} %iota_add_fusion.1, pred[1024]{0:T(1024)(128)(4,1)S(1)} %get-tuple-element.14, pred[1024]{0:T(1024)(128)(4,1)S(1)} %get-tuple-element.15), kind=kLoop, calls=%fused_computation.9 | loop fusion | flops 3932160 | bytes 795648 | tf_op jit(solution)/shard_map/and | solution.py:34
  19.4 0.0 copy-start.1
  19.4 49.5 %all-gather.2.cloned.1.call-done = bf16[768,2048]{1,0:T(8,128)(2,1)} async-done(((bf16[192,2048]{1,0:T(8,128)(2,1)}), bf16[768,2048]{1,0:T(8,128)(2,1)}) %all-gather.2.cloned.1.call-update) | async-done | bytes 3145744 | tf_op jit(solution)/shard_map/all_gather | solution.py:95
  68.9 4.1 %convolution_convert_fusion.1 = bf16[768,640]{0,1:T(8,128)(2,1)S(1)} fusion(bf16[768,2048]{1,0:T(8,128)(2,1)} %all-gather.2.cloned.1.call-done, bf16[2048,640]{1,0:T(8,128)(2,1)S(1)} %concatenate.13), kind=kOutput, calls=%fused_computation.16 | convolution fusion | flops 2013757440 | bytes 6750208 | tf_op jit(solution)/shard_map/dot_general | solution.py:94
  73.2 3.8 %collective-permute-start = (bf16[128,256]{0,1:T(8,128)(2,1)S(1)}, bf16[128,256]{0,1:T(8,128)(2,1)S(1)}, u32[]{:S(2)}, u32[]{:S(2)}) collective-permute-start(bf16[128,256]{0,1:T(8,128)(2,1)S(1)} %get-tuple-element.7), channel_id=1, source_target_pairs={{0,4},{4,8},{8,12},{12,16},{16,20},{20,24},{24,28},{28,32},{32,36}... | collective-permute-start | bytes 196616 | tf_op jit(solution)/shard_map/ppermute | solution.py:17
  77.0 1.9 %collective-permute-start.1 = (bf16[128,256]{0,1:T(8,128)(2,1)S(1)}, bf16[128,256]{0,1:T(8,128)(2,1)S(1)}, u32[]{:S(2)}, u32[]{:S(2)}) collective-permute-start(bf16[128,256]{0,1:T(8,128)(2,1)S(1)} %get-tuple-element.8), channel_id=1, source_target_pairs={{4,0},{8,4},{12,8},{16,12},{20,16},{24,20},{28,24},{32,28},{36,32}... | collective-permute-start | bytes 196616 | tf_op jit(solution)/shard_map/ppermute | solution.py:20
  78.9 0.0 copy-done.1
  79.0 0.0 collective-permute-done
  79.0 3.6 %collective-permute-done.1 = bf16[128,256]{0,1:T(8,128)(2,1)S(1)} collective-permute-done((bf16[128,256]{0,1:T(8,128)(2,1)S(1)}, bf16[128,256]{0,1:T(8,128)(2,1)S(1)}, u32[]{:S(2)}, u32[]{:S(2)}) %collective-permute-start.1) | collective-permute-done | bytes 65568 | tf_op jit(solution)/shard_map/ppermute | solution.py:20
  82.6 0.1 fusion.22
  82.8 0.3 fusion.17
  83.1 0.8 copy.26
  83.9 0.0 copy-start
  83.9 3.5 %all-to-all-start.1 = ((bf16[4,192,128]{2,1,0:T(8,128)(2,1)}), bf16[4,192,128]{2,1,0:T(8,128)(2,1)S(1)}, u32[]{:S(2)}, u32[]{:S(2)}) async-start(bf16[4,192,128]{2,1,0:T(8,128)(2,1)} %bitcast.12), calls=%async_computation.1 | async-start | bytes 393216 | tf_op jit(solution)/shard_map/all_to_all | solution.py:132
  87.4 1.4 %fusion.1 = (f32[2,768]{1,0:T(2,128)S(1)}, f32[1024,768,2]{1,0,2:T(8,128)S(1)}) fusion(pred[768,1024]{0,1:T(8,128)(4,1)S(1)} %fusion.5, bf16[768,2,64]{0,2,1:T(8,128)(2,1)S(1)} %bitcast.64, bf16[128,256]{0,1:T(8,128)(2,1)S(1)} %collective-permute-done.1, bf16[128,256]{0,1:T(8,128)(2,1)S(1)} %collective-permute-done, ...), kind=kOutput, calls=%fused_computation.4 | convolution fusion | flops 206567936 | bytes 7804928 | tf_op jit(solution)/shard_map/yxpz,ixz->xpyi/dot_general | solution.py:28
  88.8 0.0 copy-done
  88.8 0.1 broadcast_maximum_fusion
  88.9 1.5 %fusion = f32[2,768]{1,0:T(2,128)S(1)} fusion(f32[1024,768,2]{1,0,2:T(8,128)S(1)} %get-tuple-element.13, f32[2,768]{1,0:T(2,128)S(1)} %broadcast_maximum_fusion, pred[768,1024]{0,1:T(8,128)(4,1)S(1)} %fusion.5), kind=kLoop, calls=%fused_computation.3 | loop fusion | flops 6289920 | bytes 7090176 | tf_op jit(solution)/shard_map/reduce_sum | solution.py:42
  90.3 0.1 exponential_add_fusion
  90.4 2.1 %fusion.12 = bf16[768,1,2,64]{0,3,2,1:T(8,128)(2,1)S(1)} fusion(f32[2,768]{1,0:T(2,128)S(1)} %exponential_add_fusion, f32[2,768]{1,0:T(2,128)S(1)} %broadcast_maximum_fusion, f32[1024,768,2]{1,0,2:T(8,128)S(1)} %get-tuple-element.13, pred[768,1024]{0,1:T(8,128)(4,1)S(1)} %fusion.5, bf16[128,256]{0,1:T(8,128)(2,1)S(1)} %collective-permute-done.1, ...), kind=kOutput, calls=%fused_computation.18 | convolution fusion | flops 209813504 | bytes 7811072 | tf_op jit(solution)/shard_map/bhcv,vbn->cbhn/dot_general | solution.py:44
  92.5 0.3 convert_element_type.56
  92.7 0.9 copy.24
  93.6 0.0 all-to-all-done.1
  93.6 4.2 %all-to-all-start = ((bf16[4,192,128]{2,1,0:T(8,128)(2,1)}), bf16[4,192,128]{2,1,0:T(8,128)(2,1)S(1)}, u32[]{:S(2)}, u32[]{:S(2)}) async-start(bf16[4,192,128]{2,1,0:T(8,128)(2,1)} %copy.24), calls=%async_computation | async-start | bytes 393216 | tf_op jit(solution)/shard_map/all_to_all | solution.py:131
  97.8 5.2 %all-to-all-done = bf16[4,192,128]{2,1,0:T(8,128)(2,1)S(1)} async-done(((bf16[4,192,128]{2,1,0:T(8,128)(2,1)}), bf16[4,192,128]{2,1,0:T(8,128)(2,1)S(1)}, u32[]{:S(2)}, u32[]{:S(2)}) %all-to-all-start) | async-done | bytes 196640 | tf_op jit(solution)/shard_map/all_to_all | solution.py:131
  103.0 4.1 %convolution_convert_fusion = bf16[192,2048]{1,0:T(8,128)(2,1)} fusion(bf16[1024,2048]{1,0:T(8,128)(2,1)} %param.21, bf16[192,512]{1,0:T(8,128)(2,1)S(1)} %copy_bitcast_fusion, bf16[192,512]{1,0:T(8,128)(2,1)S(1)} %copy_bitcast_fusion.1), kind=kOutput, calls=%fused_computation.10 | convolution fusion | flops 806486016 | bytes 5373952 | tf_op jit(solution)/shard_map/dot_general | solution.py:135
  (10 shorter events, 0.2 us)
Async XLA Ops:
  6.5 62.4 %all-gather.2.cloned.1.call-start = ((), (), s32[]{:S(2)}) async-start(), calls=%async_computation.2 | async-start | bytes 3932160 | tf_op jit(solution)/shard_map/all_gather | solution.py:95
  19.4 59.5 %copy-start.1 = (f32[3,128]{1,0:T(4,128)S(1)}, f32[3,128]{1,0:T(4,128)}, u32[]{:S(2)}) copy-start(f32[3,128]{1,0:T(4,128)} %param.20) | copy-start | bytes 4612
  73.2 5.8 %collective-permute-start = (bf16[128,256]{0,1:T(8,128)(2,1)S(1)}, bf16[128,256]{0,1:T(8,128)(2,1)S(1)}, u32[]{:S(2)}, u32[]{:S(2)}) collective-permute-start(bf16[128,256]{0,1:T(8,128)(2,1)S(1)} %get-tuple-element.7), channel_id=1, source_target_pairs={{0,4},{4,8},{8,12},{12,16},{16,20},{20,24},{24,28},{28,32},{32,36}... | collective-permute-start | bytes 196616 | tf_op jit(solution)/shard_map/ppermute | solution.py:17
  77.0 5.6 %collective-permute-start.1 = (bf16[128,256]{0,1:T(8,128)(2,1)S(1)}, bf16[128,256]{0,1:T(8,128)(2,1)S(1)}, u32[]{:S(2)}, u32[]{:S(2)}) collective-permute-start(bf16[128,256]{0,1:T(8,128)(2,1)S(1)} %get-tuple-element.8), channel_id=1, source_target_pairs={{4,0},{8,4},{12,8},{16,12},{20,16},{24,20},{28,24},{32,28},{36,32}... | collective-permute-start | bytes 196616 | tf_op jit(solution)/shard_map/ppermute | solution.py:20
  83.9 4.9 %copy-start = (f32[2]{0:T(128)S(1)}, f32[2]{0:T(128)}, u32[]{:S(2)}) copy-start(f32[2]{0:T(128)} %param.16) | copy-start | bytes 28
  83.9 9.7 %all-to-all-start.1 = ((bf16[4,192,128]{2,1,0:T(8,128)(2,1)}), bf16[4,192,128]{2,1,0:T(8,128)(2,1)S(1)}, u32[]{:S(2)}, u32[]{:S(2)}) async-start(bf16[4,192,128]{2,1,0:T(8,128)(2,1)} %bitcast.12), calls=%async_computation.1 | async-start | bytes 393216 | tf_op jit(solution)/shard_map/all_to_all | solution.py:132
  93.6 9.4 %all-to-all-start = ((bf16[4,192,128]{2,1,0:T(8,128)(2,1)}), bf16[4,192,128]{2,1,0:T(8,128)(2,1)S(1)}, u32[]{:S(2)}, u32[]{:S(2)}) async-start(bf16[4,192,128]{2,1,0:T(8,128)(2,1)} %copy.24), calls=%async_computation | async-start | bytes 393216 | tf_op jit(solution)/shard_map/all_to_all | solution.py:131
Sparse Core Ops, SparseCore 0:
  10.3 58.5 all-gather.1
where the time goes:
time: 116 us; the launch traced here: 114 us
  waiting for transfers between devices  58.3 us (50%)
  between operations  13.6 us (12%)
  starting transfers between devices  13.5 us (12%)
  matrix products  11.7 us (10%)
  local copies, waits for them, and re-layouts  9.78 us (8%)
  other arithmetic  7.21 us (6%)
    all_gather x1, waiting for transfers between devices, body(): lax.all_gather(normed, 'tp', axis=0, tiled=True)  49.5 us
    all_to_all x1, waiting for transfers between devices, body(): lax.all_to_all(attended, 'tp', split_axis=0, concat_axis=1, tiled=True)  5.15 us
    concatenate x1, local copies, waits for them, and re-layouts, body(): jnp.concatenate([query_weight, key_weight, value_weight, conv_gate_weight...  4.58 us
    all_to_all x1, starting transfers between devices, body(): lax.all_to_all(attended, 'tp', split_axis=0, concat_axis=1, tiled=True)  4.19 us
    dot_general x1, matrix products, body(): jnp.dot(lax.all_gather(normed, 'tp', axis=0, tiled=True), all_weight, pre...  4.13 us
    dot_general x1, matrix products, body(): jnp.dot(joined, out_weight, preferred_element_type=jnp.float32)  4.09 us
    ppermute x1, starting transfers between devices, extended(): lax.ppermute(lax.slice_in_dim(block, block.shape[dim] - width, None, axis...  3.84 us
    ppermute x1, waiting for transfers between devices, extended(): lax.ppermute(lax.slice_in_dim(block, 0, width, axis=dim), axis, backward)  3.62 us
  transfers between devices with their start and end apart: 5, of which 3 were waited for; matrix products, arithmetic and copies ran while one was open for 13% of the time, Pallas kernels for 0%

commit v1 on v0

v1 whole, which is shorter than its diff:
```python
import jax
import jax.numpy as jnp
from jax import lax
from jax.experimental import pallas as pl
from jax.experimental.pallas import tpu as pltpu
from jax.sharding import PartitionSpec as P

HEAD = 64
WIN = 128
EDGE = 16
LANES = 128
F32 = jnp.float32
BF16 = jnp.bfloat16
VMEM = pl.BlockSpec(memory_space=pltpu.VMEM)
SMEM = pl.BlockSpec(memory_space=pltpu.SMEM)


def near_memory(*arrays):
    return tuple(pltpu.with_memory_space_constraint(array, pltpu.VMEM) for array in arrays)


def params(mebibytes):
    return pltpu.CompilerParams(vmem_limit_bytes=mebibytes << 20)


def split_kernel(tokens_ref, top_ref, bottom_ref, sems):
    half = top_ref.shape[0]
    copies = [
        pltpu.make_async_copy(tokens_ref.at[pl.ds(part * half, half)], ref, sems.at[part])
        for part, ref in enumerate((top_ref, bottom_ref))
    ]
    for copy in copies:
        copy.start()
    for copy in copies:
        copy.wait()


def pack_kernel(q_ref, k_ref, v_ref, gate_ref, pre_ref, input_ref, cols_ref, rows_ref):
    for place, ref in enumerate((q_ref, gate_ref, pre_ref, input_ref)):
        cols_ref[:, place * LANES : (place + 1) * LANES] = ref[...]
    for place, ref in enumerate((k_ref, k_ref, v_ref, v_ref)):
        rows_ref[place * HEAD : (place + 1) * HEAD, :] = ref[...]


def project(rows, gain, cols, kv_rows, out_ref, start):
    count = rows.shape[0]
    rows = rows.astype(F32)
    scale = lax.rsqrt(jnp.mean(rows * rows, axis=-1, keepdims=True) + 1e-06)
    normed = (rows * scale * gain).astype(BF16)
    out = jnp.dot(normed, cols, preferred_element_type=F32).astype(BF16)
    product = out[:, 2 * LANES : 3 * LANES].astype(F32) * out[:, 3 * LANES :].astype(F32)
    pairs = lax.dot_general(normed, kv_rows, (((1,), (1,)), ((), ())), preferred_element_type=F32)
    out_ref[pl.ds(start, count), : 2 * LANES] = out[:, : 2 * LANES]
    out_ref[pl.ds(start, count), 2 * LANES : 3 * LANES] = product.astype(BF16)
    out_ref[pl.ds(start, count), 3 * LANES :] = pairs.astype(BF16)


def near_kernel(top_ref, bottom_ref, at_ref, ab_ref, bt_ref, bb_ref, gain_ref, cols_ref, rows_ref, out_ref):
    gain, cols, rows = gain_ref[...], cols_ref[...], rows_ref[...]
    for place, ref in enumerate((top_ref, bottom_ref, at_ref, ab_ref, bt_ref, bb_ref)):
        project(ref[...], gain, cols, rows, out_ref, place * ref.shape[0])


def far_kernel(near_ref, ot_ref, ob_ref, gain_ref, cols_ref, rows_ref, full_ref, head_ref, tail_ref):
    chunk = near_ref.shape[0] // 3
    half = chunk // 2
    total = full_ref.shape[0]
    place = lax.axis_index("tp")
    for slot, shift in enumerate((0, 3, 1)):
        start = pl.multiple_of(lax.rem(place + shift, 4) * chunk, 64)
        full_ref[pl.ds(start, chunk), :] = near_ref[slot * chunk : (slot + 1) * chunk, :]
    gain, cols, rows = gain_ref[...], cols_ref[...], rows_ref[...]
    for part, ref in enumerate((ot_ref, ob_ref)):
        start = pl.multiple_of(lax.rem(place + 2, 4) * chunk + part * half, 32)
        project(ref[...], gain, cols, rows, full_ref, start)
    lane = lax.broadcasted_iota(jnp.int32, (WIN, LANES), 1)
    for ref, rows, edge in ((head_ref, 0, 0), (tail_ref, total - WIN, total - EDGE)):
        keys = full_ref[rows : rows + WIN, 3 * LANES : 4 * LANES].astype(F32)
        values = full_ref[rows : rows + WIN, 4 * LANES :].astype(F32)
        ref[:WIN, :] = jnp.where(lane < HEAD, keys, values).astype(BF16)
        ref[WIN:, :] = full_ref[edge : edge + EDGE, 2 * LANES : 3 * LANES]


def mix_kernel(sink_ref, taps_ref, full_ref, low_ref, high_ref, out_ref, key_ref, value_ref, conv_ref, *, last):
    total = full_ref.shape[0]
    lane = lax.broadcasted_iota(jnp.int32, (WIN, LANES), 1)
    for ref, row in ((low_ref, 0), (high_ref, WIN + total)):
        pair = ref[:WIN, :].astype(F32)
        turned = pltpu.roll(pair, HEAD, 1)
        key_ref[row : row + WIN, :] = jnp.where(lane < HEAD, pair, turned).astype(BF16)
        value_ref[row : row + WIN, :] = jnp.where(lane < HEAD, turned, pair).astype(BF16)
    key_ref[WIN : WIN + total, :] = full_ref[:, 3 * LANES : 4 * LANES]
    value_ref[WIN : WIN + total, :] = full_ref[:, 4 * LANES :]

    conv_ref[0:8, :] = low_ref[WIN + EDGE - 8 :, :].astype(F32)
    conv_ref[8 : 8 + total, :] = full_ref[:, 2 * LANES : 3 * LANES].astype(F32)
    conv_ref[8 + total :, :] = high_ref[WIN : WIN + 8, :].astype(F32)
    convolved = (
        taps_ref[0:1, :] * conv_ref[7 : 7 + total, :]
        + taps_ref[1:2, :] * conv_ref[8 : 8 + total, :]
        + taps_ref[2:3, :] * conv_ref[9 : 9 + total, :]
    )
    gate = full_ref[:, LANES : 2 * LANES].astype(F32)
    out_ref[:, LANES:] = (gate * convolved).astype(BF16)

    place = lax.axis_index("sp")
    row = lax.broadcasted_iota(jnp.int32, (2 * WIN, 3 * WIN), 0)
    col = lax.broadcasted_iota(jnp.int32, (2 * WIN, 3 * WIN), 1)
    rel = col - lax.rem(row, WIN)
    band = (rel >= 0) & (rel <= 2 * WIN)
    half = lax.broadcasted_iota(jnp.int32, (2 * WIN, 1), 0) < WIN
    sink = jnp.where(half, sink_ref[0], sink_ref[1])
    blocks = total // WIN
    for block in range(blocks):
        at = block * WIN
        query = full_ref[at : at + WIN, :LANES]
        zero = jnp.zeros_like(query)
        both = jnp.concatenate([jnp.where(lane < HEAD, query, zero), jnp.where(lane < HEAD, zero, query)], axis=0)
        score = lax.dot_general(
            both, key_ref[at : at + 3 * WIN, :], (((1,), (1,)), ((), ())), preferred_element_type=F32
        ) * HEAD ** (-0.5)
        allowed = band
        if block == 0:
            allowed = allowed & (col >= jnp.where(place == 0, WIN, 0))
        if block == blocks - 1:
            allowed = allowed & (col < jnp.where(place == last, 2 * WIN, 3 * WIN))
        score = jnp.where(allowed, score, -jnp.inf)
        top = jnp.maximum(jnp.max(score, axis=-1, keepdims=True), sink)
        expo = jnp.exp(score - top)
        denom = jnp.sum(expo, axis=-1, keepdims=True) + jnp.exp(sink - top)
        weights = (expo * (1.0 / denom)).astype(BF16)
        got = jnp.dot(weights, value_ref[at : at + 3 * WIN, :], preferred_element_type=F32)
        out_ref[at : at + WIN, :LANES] = jnp.where(lane < HEAD, got[:WIN], got[WIN:]).astype(BF16)


def out_kernel(parts_ref, weight_ref, out_ref):
    count = parts_ref.shape[0]
    joined = jnp.concatenate(
        [parts_ref[i, :, :LANES] for i in range(count)] + [parts_ref[i, :, LANES:] for i in range(count)], axis=1
    )
    out_ref[...] = jnp.dot(joined, weight_ref[...], preferred_element_type=F32).astype(BF16)


def body(
    tokens,
    norm_gain,
    query_weight,
    key_weight,
    value_weight,
    sink_logit,
    conv_gate_weight,
    conv_pre_weight,
    conv_input_weight,
    conv_taps,
    out_weight,
):
    chunk, width = tokens.shape
    total = 4 * chunk
    half = chunk // 2
    forward = [(i, (i + 1) % 4) for i in range(4)]
    backward = [(i, (i + 3) % 4) for i in range(4)]
    top, bottom = pl.pallas_call(
        split_kernel,
        name="split",
        out_shape=(pltpu.VMEM((half, width), BF16), pltpu.VMEM((half, width), BF16)),
        in_specs=[pl.BlockSpec(memory_space=pltpu.HBM)],
        out_specs=(VMEM, VMEM),
        scratch_shapes=[pltpu.SemaphoreType.DMA((2,))],
        compiler_params=params(16),
    )(pltpu.with_memory_space_constraint(tokens, pltpu.HBM))
    before_top = lax.ppermute(top, "tp", forward)
    after_bottom = lax.ppermute(bottom, "tp", backward)
    before_bottom = lax.ppermute(bottom, "tp", forward)
    after_top = lax.ppermute(top, "tp", backward)
    far_top = lax.ppermute(before_top, "tp", forward)
    far_bottom = lax.ppermute(after_bottom, "tp", backward)

    cols, rows = pl.pallas_call(
        pack_kernel,
        name="pack",
        out_shape=(pltpu.VMEM((width, 4 * LANES), BF16), pltpu.VMEM((2 * LANES, width), BF16)),
        in_specs=[VMEM] * 6,
        out_specs=(VMEM, VMEM),
        compiler_params=params(16),
    )(query_weight, key_weight.T, value_weight.T, conv_gate_weight, conv_pre_weight, conv_input_weight)
    gain = norm_gain.reshape(1, width)
    near = pl.pallas_call(
        near_kernel,
        name="near",
        out_shape=pltpu.VMEM((3 * chunk, 5 * LANES), BF16),
        in_specs=[VMEM] * 9,
        out_specs=VMEM,
        compiler_params=params(16),
    )(*near_memory(top, bottom, before_top, before_bottom, after_top, after_bottom, gain, cols, rows))
    full, head, tail = pl.pallas_call(
        far_kernel,
        name="far",
        out_shape=(
            pltpu.VMEM((total, 5 * LANES), BF16),
            pltpu.VMEM((WIN + EDGE, LANES), BF16),
            pltpu.VMEM((WIN + EDGE, LANES), BF16),
        ),
        in_specs=[VMEM] * 6,
        out_specs=(VMEM, VMEM, VMEM),
        compiler_params=params(16),
    )(*near_memory(near, far_top, far_bottom, gain, cols, rows))

    count = lax.axis_size("sp")
    up = [(i, i + 1) for i in range(count - 1)]
    down = [(i + 1, i) for i in range(count - 1)]
    low = lax.ppermute(tail, "sp", up)
    high = lax.ppermute(head, "sp", down)

    def mix(*refs):
        mix_kernel(*refs, last=count - 1)

    mixed = pl.pallas_call(
        mix,
        name="mix",
        out_shape=pltpu.VMEM((total, 2 * LANES), BF16),
        in_specs=[SMEM] + [VMEM] * 4,
        compiler_params=params(16),
        out_specs=VMEM,
        scratch_shapes=[
            pltpu.VMEM((total + 2 * WIN, LANES), BF16),
            pltpu.VMEM((total + 2 * WIN, LANES), BF16),
            pltpu.VMEM((total + 16, LANES), F32),
        ],
    )(sink_logit, *near_memory(conv_taps, full, low, high))
    parts = lax.all_to_all(mixed.reshape(4, chunk, 2 * LANES), "tp", split_axis=0, concat_axis=0, tiled=True)
    step = 512
    parts, out_weight = near_memory(parts, out_weight)
    return pl.pallas_call(
        out_kernel,
        name="project_out",
        out_shape=jax.ShapeDtypeStruct((chunk, out_weight.shape[1]), BF16),
        grid=(out_weight.shape[1] // step,),
        in_specs=[
            pl.BlockSpec((4, chunk, 2 * LANES), lambda i: (0, 0, 0)),
            pl.BlockSpec((out_weight.shape[0], step), lambda i: (0, i)),
        ],
        out_specs=pl.BlockSpec((chunk, step), lambda i: (0, i)),
        compiler_params=params(16),
    )(parts, out_weight)


def solution(mesh):
    placed = (
        P(("sp", "tp"), None),
        P(),
        P(None, "tp"),
        P(None, "tp"),
        P(None, "tp"),
        P("tp"),
        P(None, "tp"),
        P(None, "tp"),
        P(None, "tp"),
        P(None, "tp"),
        P(),
    )
    return jax.shard_map(
        body, mesh=mesh, in_specs=placed, out_specs=P(("sp", "tp"), None), check_vma=False
    )
```

time: 116 us -> 70.5 us (0.61); the launches traced: 114 us -> 69.8 us
  waiting for transfers between devices: 58.3 us -> 0.85 us
  starting transfers between devices: 13.5 us -> 38.5 us
  between operations: 13.6 us -> 0.18 us
  Pallas kernels: 0 us -> 13.3 us
  matrix products: 11.7 us -> 0 us
  blocking collectives: 0 us -> 10.2 us
  other arithmetic: 7.21 us -> 0 us
  local copies, waits for them, and re-layouts: 9.78 us -> 6.76 us
    all_gather x1 -> x0, waiting for transfers between devices: 49.5 us -> none  [body(): lax.all_gather(normed, 'tp', axis=0, tiled=True)]
    ppermute x2 -> x8, starting transfers between devices: 5.76 us -> 38.5 us  [the longest x1 11.8 us: body(): high = lax.ppermute(head, 'sp', down)]
    pallas_call x0 -> x6, Pallas kernels: none -> 13.3 us  [the longest x1 3.98 us: body(): pl.pallas_call(near_kernel, name='near', out_shape=pltpu.VMEM((3 * chunk,...]
    dot_general x4 -> x0, matrix products: 11.7 us -> none  [the longest x1 4.13 us: body(): jnp.dot(lax.all_gather(normed, 'tp', axis=0, tiled=True), all_weight, pre...]
    all_to_all x0 -> x1, blocking collectives: none -> 10.2 us  [body(): lax.all_to_all(mixed.reshape(4, chunk, 2 * LANES), 'tp', split_axis=0, co...]
    all_to_all x2 -> x0, starting transfers between devices: 7.69 us -> none  [the longest x1 4.19 us: body(): lax.all_to_all(attended, 'tp', split_axis=0, concat_axis=1, tiled=True)]
    all_to_all x2 -> x0, waiting for transfers between devices: 5.15 us -> none  [the longest x1 5.15 us: body(): lax.all_to_all(attended, 'tp', split_axis=0, concat_axis=1, tiled=True)]
    concatenate x1 -> x0, local copies, waits for them, and re-layouts: 4.58 us -> none  [body(): jnp.concatenate([query_weight, key_weight, value_weight, conv_gate_weight...]
  transfers between devices with their start and end apart: 5 -> 8, of which waited for: 3 -> 1; matrix products, arithmetic and copies ran while one was open for 13% -> 0% of each run, Pallas kernels for 0% -> 6%
where the time goes in v1:
time: 70.5 us; the launch traced here: 69.8 us
  starting transfers between devices  38.5 us (55%)
  Pallas kernels  13.3 us (19%)
  blocking collectives  10.2 us (14%)
  local copies, waits for them, and re-layouts  6.76 us (10%)
  waiting for transfers between devices  0.85 us (1%)
    ppermute x1, starting transfers between devices, body(): high = lax.ppermute(head, 'sp', down)  11.8 us
    all_to_all x1, blocking collectives, body(): lax.all_to_all(mixed.reshape(4, chunk, 2 * LANES), 'tp', split_axis=0, co...  10.2 us
    unnamed x20, local copies, waits for them, and re-layouts  6.76 us
    ppermute x1, starting transfers between devices, body(): low = lax.ppermute(tail, 'sp', up)  6.56 us
    ppermute x1, starting transfers between devices, body(): far_bottom = lax.ppermute(after_bottom, 'tp', backward)  4.57 us
    ppermute x1, starting transfers between devices, body(): after_top = lax.ppermute(top, 'tp', backward)  4.4 us
    pallas_call x1, Pallas kernels, body(): pl.pallas_call(near_kernel, name='near', out_shape=pltpu.VMEM((3 * chunk,...  3.98 us
    ppermute x1, starting transfers between devices, body(): before_top = lax.ppermute(top, 'tp', forward)  3.94 us
  transfers between devices with their start and end apart: 8, of which 1 were waited for; matrix products, arithmetic and copies ran while one was open for 0% of the time, Pallas kernels for 6%

profile of v1, /device:TPU:1, one launch (start us, length us, event | category | flops | bytes accessed | tf_op | source)
XLA Modules:
  0.0 69.8 jit_solution(13949289186853081957)
XLA Ops:
  0.0 1.1 %split.1 = (bf16[96,2048]{1,0:T(8,128)(2,1)S(1)}, bf16[96,2048]{1,0:T(8,128)(2,1)S(1)}) custom-call(bf16[192,2048]{1,0:T(8,128)(2,1)} %tokens_ref.1), custom_call_target="tpu_custom_call" | custom-call | tf_op jit(solution)/shard_map/split/pallas_call | solution.py:162
  1.1 3.9 %collective-permute-start = (bf16[96,2048]{1,0:T(8,128)(2,1)S(1)}, bf16[96,2048]{1,0:T(8,128)(2,1)S(1)}, u32[]{:S(2)}, u32[]{:S(2)}) collective-permute-start(bf16[96,2048]{1,0:T(8,128)(2,1)S(1)} %get-tuple-element.12.top_ref), channel_id=1, source_target_pairs={{0,1},{1,2},{2,3},{3,0},{4,5},{5,6},{6,7},{7,4},{8,9},{9,10},{10,1... | collective-permute-start | bytes 1179656 | tf_op jit(solution)/shard_map/ppermute | solution.py:171
  5.1 3.2 %collective-permute-start.3 = (bf16[96,2048]{1,0:T(8,128)(2,1)S(1)}, bf16[96,2048]{1,0:T(8,128)(2,1)S(1)}, u32[]{:S(2)}, u32[]{:S(2)}) collective-permute-start(bf16[96,2048]{1,0:T(8,128)(2,1)S(1)} %get-tuple-element.13.bottom_ref), channel_id=1, source_target_pairs={{0,3},{1,0},{2,1},{3,2},{4,7},{5,4},{6,5},{7,6},{8,11},{9,8},{10,9... | collective-permute-start | bytes 1179656 | tf_op jit(solution)/shard_map/ppermute | solution.py:172
  8.3 2.1 %collective-permute-start.1 = (bf16[96,2048]{1,0:T(8,128)(2,1)S(1)}, bf16[96,2048]{1,0:T(8,128)(2,1)S(1)}, u32[]{:S(2)}, u32[]{:S(2)}) collective-permute-start(bf16[96,2048]{1,0:T(8,128)(2,1)S(1)} %get-tuple-element.13.bottom_ref), channel_id=1, source_target_pairs={{0,1},{1,2},{2,3},{3,0},{4,5},{5,6},{6,7},{7,4},{8,9},{9,10},{10,1... | collective-permute-start | bytes 1179656 | tf_op jit(solution)/shard_map/ppermute | solution.py:173
  10.4 4.4 %collective-permute-start.2 = (bf16[96,2048]{1,0:T(8,128)(2,1)S(1)}, bf16[96,2048]{1,0:T(8,128)(2,1)S(1)}, u32[]{:S(2)}, u32[]{:S(2)}) collective-permute-start(bf16[96,2048]{1,0:T(8,128)(2,1)S(1)} %get-tuple-element.12.top_ref), channel_id=1, source_target_pairs={{0,3},{1,0},{2,1},{3,2},{4,7},{5,4},{6,5},{7,6},{8,11},{9,8},{10,9... | collective-permute-start | bytes 1179656 | tf_op jit(solution)/shard_map/ppermute | solution.py:174
  14.8 0.0 collective-permute-done.at_ref
  14.8 1.9 %collective-permute-start.4 = (bf16[96,2048]{1,0:T(8,128)(2,1)S(1)}, bf16[96,2048]{1,0:T(8,128)(2,1)S(1)}, u32[]{:S(2)}, u32[]{:S(2)}) collective-permute-start(bf16[96,2048]{1,0:T(8,128)(2,1)S(1)} %collective-permute-done.at_ref), channel_id=1, source_target_pairs={{0,1},{1,2},{2,3},{3,0},{4,5},{5,6},{6,7},{7,4},{8,9},{9,10},{10,1... | collective-permute-start | bytes 1179656 | tf_op jit(solution)/shard_map/ppermute | solution.py:175
  16.7 0.0 collective-permute-done.3.bb_ref
  16.7 4.6 %collective-permute-start.5 = (bf16[96,2048]{1,0:T(8,128)(2,1)S(1)}, bf16[96,2048]{1,0:T(8,128)(2,1)S(1)}, u32[]{:S(2)}, u32[]{:S(2)}) collective-permute-start(bf16[96,2048]{1,0:T(8,128)(2,1)S(1)} %collective-permute-done.3.bb_ref), channel_id=1, source_target_pairs={{0,3},{1,0},{2,1},{3,2},{4,7},{5,4},{6,5},{7,6},{8,11},{9,8},{10,9... | collective-permute-start | bytes 1179656 | tf_op jit(solution)/shard_map/ppermute | solution.py:176
  21.3 0.0 copy-start.1
  21.3 1.0 %copy-done.1 = bf16[2048,128]{1,0:T(8,128)(2,1)S(1)} copy-done((bf16[2048,128]{1,0:T(8,128)(2,1)S(1)}, bf16[2048,128]{1,0:T(8,128)(2,1)}, u32[]{:S(2)}) %copy-start.1) | copy-done | bytes 524312
  22.4 0.0 copy-start.2
  22.4 1.0 %copy-done.2 = bf16[2048,128]{1,0:T(8,128)(2,1)S(1)} copy-done((bf16[2048,128]{1,0:T(8,128)(2,1)S(1)}, bf16[2048,128]{1,0:T(8,128)(2,1)}, u32[]{:S(2)}) %copy-start.2) | copy-done | bytes 524312
  23.4 0.0 copy-start.3
  23.4 1.0 %copy-done.3 = bf16[2048,128]{1,0:T(8,128)(2,1)S(1)} copy-done((bf16[2048,128]{1,0:T(8,128)(2,1)S(1)}, bf16[2048,128]{1,0:T(8,128)(2,1)}, u32[]{:S(2)}) %copy-start.3) | copy-done | bytes 524312
  24.4 0.0 copy-start.4
  24.4 1.0 %copy-done.4 = bf16[2048,128]{1,0:T(8,128)(2,1)S(1)} copy-done((bf16[2048,128]{1,0:T(8,128)(2,1)S(1)}, bf16[2048,128]{1,0:T(8,128)(2,1)}, u32[]{:S(2)}) %copy-start.4) | copy-done | bytes 524312
  25.5 0.0 copy-start.5
  25.5 0.9 %copy-done.5 = bf16[2048,64]{0,1:T(8,128)(2,1)S(1)} copy-done((bf16[2048,64]{0,1:T(8,128)(2,1)S(1)}, bf16[2048,64]{0,1:T(8,128)(2,1)}, u32[]{:S(2)}) %copy-start.5) | copy-done | bytes 262168
  26.4 0.0 copy-start.6
  26.4 0.9 %copy-done.6 = bf16[2048,64]{0,1:T(8,128)(2,1)S(1)} copy-done((bf16[2048,64]{0,1:T(8,128)(2,1)S(1)}, bf16[2048,64]{0,1:T(8,128)(2,1)}, u32[]{:S(2)}) %copy-start.6) | copy-done | bytes 262168
  27.4 0.4 pack.1
  27.8 0.0 collective-permute-done.1.ab_ref
  27.8 0.0 collective-permute-done.2.bt_ref
  27.8 0.0 copy-start.7
  27.9 0.7 copy-done.7
  28.5 0.0 copy-start.8
  28.5 0.0 copy-start.9
  28.5 4.0 %near.1.near_ref = bf16[576,640]{1,0:T(8,128)(2,1)S(1)} custom-call(bf16[96,2048]{1,0:T(8,128)(2,1)S(1)} %get-tuple-element.12.top_ref, bf16[96,2048]{1,0:T(8,128)(2,1)S(1)} %get-tuple-element.13.bottom_ref, bf16[96,2048]{1,0:T(8,128)(2,1)S(1)} %collective-permute-done.at_ref, bf16[96,2048]{1,0:T(8,128)(2,1)S(1)} %collective-permute-done.1.ab_ref, ...), custom_call_target="tpu_custom_call" | custom-call | tf_op jit(solution)/shard_map/near/pallas_call | solution.py:187
  32.5 0.0 copy-start
  32.5 0.0 collective-permute-done.4.ot_ref
  32.6 0.0 collective-permute-done.5.ob_ref
  32.6 1.6 %far.1 = (bf16[768,640]{1,0:T(8,128)(2,1)S(1)}, bf16[144,128]{1,0:T(8,128)(2,1)S(1)}, bf16[144,128]{1,0:T(8,128)(2,1)S(1)}) custom-call(bf16[576,640]{1,0:T(8,128)(2,1)S(1)} %near.1.near_ref, bf16[96,2048]{1,0:T(8,128)(2,1)S(1)} %collective-permute-done.4.ot_ref, bf16[96,2048]{1,0:T(8,128)(2,1)S(1)} %collective-permute-done.5.ob_ref, f32[1,2048]{1,0:T(1,128)S(1)} %bitcast.8, ...), custom_call_target="tpu_custom_call" | custom-call | tf_op jit(solution)/shard_map/far/pallas_call | solution.py:195
  34.1 6.6 %collective-permute-start.6 = (bf16[144,128]{1,0:T(8,128)(2,1)S(1)}, bf16[144,128]{1,0:T(8,128)(2,1)S(1)}, u32[]{:S(2)}, u32[]{:S(2)}) collective-permute-start(bf16[144,128]{1,0:T(8,128)(2,1)S(1)} %get-tuple-element.17), channel_id=1, source_target_pairs={{0,4},{4,8},{8,12},{12,16},{16,20},{20,24},{24,28},{28,32},{32,36}... | collective-permute-start | bytes 110600 | tf_op jit(solution)/shard_map/ppermute | solution.py:211
  40.7 11.8 %collective-permute-start.7 = (bf16[144,128]{1,0:T(8,128)(2,1)S(1)}, bf16[144,128]{1,0:T(8,128)(2,1)S(1)}, u32[]{:S(2)}, u32[]{:S(2)}) collective-permute-start(bf16[144,128]{1,0:T(8,128)(2,1)S(1)} %get-tuple-element.18), channel_id=1, source_target_pairs={{4,0},{8,4},{12,8},{16,12},{20,16},{24,20},{28,24},{32,28},{36,32}... | collective-permute-start | bytes 110600 | tf_op jit(solution)/shard_map/ppermute | solution.py:212
  52.5 0.0 collective-permute-done.6.refs_3_
  52.6 0.8 %collective-permute-done.7.refs_4_ = bf16[144,128]{1,0:T(8,128)(2,1)S(1)} collective-permute-done((bf16[144,128]{1,0:T(8,128)(2,1)S(1)}, bf16[144,128]{1,0:T(8,128)(2,1)S(1)}, u32[]{:S(2)}, u32[]{:S(2)}) %collective-permute-start.7) | collective-permute-done | bytes 36896 | tf_op jit(solution)/shard_map/ppermute | solution.py:212
  53.4 0.0 copy-done.8
  53.4 0.0 copy-done.9
  53.4 3.4 %mix.1 = bf16[768,256]{1,0:T(8,128)(2,1)S(1)} custom-call(f32[2]{0:T(128)S(1)} %copy-done.9, f32[3,128]{1,0:T(4,128)S(1)} %copy-done.8, bf16[768,640]{1,0:T(8,128)(2,1)S(1)} %get-tuple-element.16.refs_2_, bf16[144,128]{1,0:T(8,128)(2,1)S(1)} %collective-permute-done.6.refs_3_, bf16[144,128]{1,0:T(8,128)(2,1)S(1)} %collective-permute-done.7.refs_4_), custom_call_target="tpu_custom_call" | custom-call | tf_op jit(solution)/shard_map/mix/pallas_call | solution.py:217
  56.8 10.2 %all_to_all.5.parts_ref = bf16[4,192,256]{2,1,0:T(8,128)(2,1)S(1)} all-to-all(bf16[4,192,256]{2,1,0:T(8,128)(2,1)S(1)} %bitcast.4), channel_id=1, replica_groups=mesh['sp'=256,'tp'=4] {'tp'}, dimensions={0} | all-to-all | bytes 786432 | tf_op jit(solution)/shard_map/all_to_all | solution.py:230
  67.1 0.0 copy-done
  67.1 2.8 %project_out.1 = bf16[192,2048]{1,0:T(8,128)(2,1)} custom-call(bf16[4,192,256]{2,1,0:T(8,128)(2,1)S(1)} %all_to_all.5.parts_ref, bf16[1024,2048]{1,0:T(8,128)(2,1)S(1)} %copy-done), custom_call_target="tpu_custom_call" | custom-call | tf_op jit(solution)/shard_map/project_out/pallas_call | solution.py:233
Async XLA Ops:
  1.1 13.7 %collective-permute-start = (bf16[96,2048]{1,0:T(8,128)(2,1)S(1)}, bf16[96,2048]{1,0:T(8,128)(2,1)S(1)}, u32[]{:S(2)}, u32[]{:S(2)}) collective-permute-start(bf16[96,2048]{1,0:T(8,128)(2,1)S(1)} %get-tuple-element.12.top_ref), channel_id=1, source_target_pairs={{0,1},{1,2},{2,3},{3,0},{4,5},{5,6},{6,7},{7,4},{8,9},{9,10},{10,1... | collective-permute-start | bytes 1179656 | tf_op jit(solution)/shard_map/ppermute | solution.py:171
  5.1 11.6 %collective-permute-start.3 = (bf16[96,2048]{1,0:T(8,128)(2,1)S(1)}, bf16[96,2048]{1,0:T(8,128)(2,1)S(1)}, u32[]{:S(2)}, u32[]{:S(2)}) collective-permute-start(bf16[96,2048]{1,0:T(8,128)(2,1)S(1)} %get-tuple-element.13.bottom_ref), channel_id=1, source_target_pairs={{0,3},{1,0},{2,1},{3,2},{4,7},{5,4},{6,5},{7,6},{8,11},{9,8},{10,9... | collective-permute-start | bytes 1179656 | tf_op jit(solution)/shard_map/ppermute | solution.py:172
  8.3 19.5 %collective-permute-start.1 = (bf16[96,2048]{1,0:T(8,128)(2,1)S(1)}, bf16[96,2048]{1,0:T(8,128)(2,1)S(1)}, u32[]{:S(2)}, u32[]{:S(2)}) collective-permute-start(bf16[96,2048]{1,0:T(8,128)(2,1)S(1)} %get-tuple-element.13.bottom_ref), channel_id=1, source_target_pairs={{0,1},{1,2},{2,3},{3,0},{4,5},{5,6},{6,7},{7,4},{8,9},{9,10},{10,1... | collective-permute-start | bytes 1179656 | tf_op jit(solution)/shard_map/ppermute | solution.py:173
  10.4 17.5 %collective-permute-start.2 = (bf16[96,2048]{1,0:T(8,128)(2,1)S(1)}, bf16[96,2048]{1,0:T(8,128)(2,1)S(1)}, u32[]{:S(2)}, u32[]{:S(2)}) collective-permute-start(bf16[96,2048]{1,0:T(8,128)(2,1)S(1)} %get-tuple-element.12.top_ref), channel_id=1, source_target_pairs={{0,3},{1,0},{2,1},{3,2},{4,7},{5,4},{6,5},{7,6},{8,11},{9,8},{10,9... | collective-permute-start | bytes 1179656 | tf_op jit(solution)/shard_map/ppermute | solution.py:174
  14.8 17.7 %collective-permute-start.4 = (bf16[96,2048]{1,0:T(8,128)(2,1)S(1)}, bf16[96,2048]{1,0:T(8,128)(2,1)S(1)}, u32[]{:S(2)}, u32[]{:S(2)}) collective-permute-start(bf16[96,2048]{1,0:T(8,128)(2,1)S(1)} %collective-permute-done.at_ref), channel_id=1, source_target_pairs={{0,1},{1,2},{2,3},{3,0},{4,5},{5,6},{6,7},{7,4},{8,9},{9,10},{10,1... | collective-permute-start | bytes 1179656 | tf_op jit(solution)/shard_map/ppermute | solution.py:175
  16.7 15.8 %collective-permute-start.5 = (bf16[96,2048]{1,0:T(8,128)(2,1)S(1)}, bf16[96,2048]{1,0:T(8,128)(2,1)S(1)}, u32[]{:S(2)}, u32[]{:S(2)}) collective-permute-start(bf16[96,2048]{1,0:T(8,128)(2,1)S(1)} %collective-permute-done.3.bb_ref), channel_id=1, source_target_pairs={{0,3},{1,0},{2,1},{3,2},{4,7},{5,4},{6,5},{7,6},{8,11},{9,8},{10,9... | collective-permute-start | bytes 1179656 | tf_op jit(solution)/shard_map/ppermute | solution.py:176
  21.3 1.0 %copy-start.1 = (bf16[2048,128]{1,0:T(8,128)(2,1)S(1)}, bf16[2048,128]{1,0:T(8,128)(2,1)}, u32[]{:S(2)}) copy-start(bf16[2048,128]{1,0:T(8,128)(2,1)} %q_ref.1) | copy-start | bytes 1572868
  22.4 1.0 %copy-start.2 = (bf16[2048,128]{1,0:T(8,128)(2,1)S(1)}, bf16[2048,128]{1,0:T(8,128)(2,1)}, u32[]{:S(2)}) copy-start(bf16[2048,128]{1,0:T(8,128)(2,1)} %gate_ref.1) | copy-start | bytes 1572868
  23.4 1.0 %copy-start.3 = (bf16[2048,128]{1,0:T(8,128)(2,1)S(1)}, bf16[2048,128]{1,0:T(8,128)(2,1)}, u32[]{:S(2)}) copy-start(bf16[2048,128]{1,0:T(8,128)(2,1)} %pre_ref.1) | copy-start | bytes 1572868
  24.4 1.0 %copy-start.4 = (bf16[2048,128]{1,0:T(8,128)(2,1)S(1)}, bf16[2048,128]{1,0:T(8,128)(2,1)}, u32[]{:S(2)}) copy-start(bf16[2048,128]{1,0:T(8,128)(2,1)} %input_ref.1) | copy-start | bytes 1572868
  25.5 0.9 %copy-start.5 = (bf16[2048,64]{0,1:T(8,128)(2,1)S(1)}, bf16[2048,64]{0,1:T(8,128)(2,1)}, u32[]{:S(2)}) copy-start(bf16[2048,64]{0,1:T(8,128)(2,1)} %param.14) | copy-start | bytes 786436
  26.4 0.9 %copy-start.6 = (bf16[2048,64]{0,1:T(8,128)(2,1)S(1)}, bf16[2048,64]{0,1:T(8,128)(2,1)}, u32[]{:S(2)}) copy-start(bf16[2048,64]{0,1:T(8,128)(2,1)} %param.15) | copy-start | bytes 786436
  27.8 0.7 %copy-start.7 = (f32[2048]{0:T(1024)S(1)}, f32[2048]{0:T(1024)}, u32[]{:S(2)}) copy-start(f32[2048]{0:T(1024)} %param.12) | copy-start | bytes 24580
  28.5 24.8 %copy-start.8 = (f32[3,128]{1,0:T(4,128)S(1)}, f32[3,128]{1,0:T(4,128)}, u32[]{:S(2)}) copy-start(f32[3,128]{1,0:T(4,128)} %refs_1_.1) | copy-start | bytes 4612
  28.5 24.8 %copy-start.9 = (f32[2]{0:T(128)S(1)}, f32[2]{0:T(128)}, u32[]{:S(2)}) copy-start(f32[2]{0:T(128)} %refs_0_.1) | copy-start | bytes 28
  32.5 34.5 %copy-start = (bf16[1024,2048]{1,0:T(8,128)(2,1)S(1)}, bf16[1024,2048]{1,0:T(8,128)(2,1)}, u32[]{:S(2)}) copy-start(bf16[1024,2048]{1,0:T(8,128)(2,1)} %weight_ref.1) | copy-start | bytes 12582916
  34.1 18.4 %collective-permute-start.6 = (bf16[144,128]{1,0:T(8,128)(2,1)S(1)}, bf16[144,128]{1,0:T(8,128)(2,1)S(1)}, u32[]{:S(2)}, u32[]{:S(2)}) collective-permute-start(bf16[144,128]{1,0:T(8,128)(2,1)S(1)} %get-tuple-element.17), channel_id=1, source_target_pairs={{0,4},{4,8},{8,12},{12,16},{16,20},{20,24},{24,28},{28,32},{32,36}... | collective-permute-start | bytes 110600 | tf_op jit(solution)/shard_map/ppermute | solution.py:211
  40.7 12.7 %collective-permute-start.7 = (bf16[144,128]{1,0:T(8,128)(2,1)S(1)}, bf16[144,128]{1,0:T(8,128)(2,1)S(1)}, u32[]{:S(2)}, u32[]{:S(2)}) collective-permute-start(bf16[144,128]{1,0:T(8,128)(2,1)S(1)} %get-tuple-element.18), channel_id=1, source_target_pairs={{4,0},{8,4},{12,8},{16,12},{20,16},{24,20},{28,24},{32,28},{36,32}... | collective-permute-start | bytes 110600 | tf_op jit(solution)/shard_map/ppermute | solution.py:212

commit v2 on v1

v2 whole, which is shorter than its diff:
```python
import jax
import jax.numpy as jnp
from jax import lax
from jax.experimental import pallas as pl
from jax.experimental.pallas import tpu as pltpu
from jax.sharding import PartitionSpec as P


HEAD = 64
WIN = 128
EDGE = 16
LANES = 128
F32 = jnp.float32
BF16 = jnp.bfloat16
VMEM = pl.BlockSpec(memory_space=pltpu.VMEM)
SMEM = pl.BlockSpec(memory_space=pltpu.SMEM)


def near_memory(*arrays):
    return tuple(pltpu.with_memory_space_constraint(array, pltpu.VMEM) for array in arrays)


def params(mebibytes):
    return pltpu.CompilerParams(vmem_limit_bytes=mebibytes << 20)


def run_copies(pairs, sems):
    copies = [pltpu.make_async_copy(source, target, sems.at[i]) for i, (source, target) in enumerate(pairs)]
    for copy in copies:
        copy.start()
    for copy in copies:
        copy.wait()


def split_kernel(tokens_ref, top_ref, bottom_ref, sems):
    rows = top_ref.shape[0]
    run_copies(
        (
            (tokens_ref.at[pl.ds(0, rows)], top_ref),
            (tokens_ref.at[pl.ds(rows, bottom_ref.shape[0])], bottom_ref),
        ),
        sems,
    )


def pack_kernel(q_ref, k_ref, v_ref, gate_ref, pre_ref, input_ref, gain_ref, cols_ref, rows_ref, gain_out_ref, sems):
    pairs = [
        (ref, cols_ref.at[:, pl.ds(place * LANES, LANES)])
        for place, ref in enumerate((q_ref, gate_ref, pre_ref, input_ref))
    ]
    pairs += [
        (ref, rows_ref.at[pl.ds(place * HEAD, HEAD)]) for place, ref in enumerate((k_ref, k_ref, v_ref, v_ref))
    ]
    run_copies(pairs + [(gain_ref, gain_out_ref)], sems)


def project(rows, gain, cols, kv_rows, out_ref, start):
    count = rows.shape[0]
    rows = rows.astype(F32)
    scale = lax.rsqrt(jnp.mean(rows * rows, axis=-1, keepdims=True) + 1e-06)
    normed = (rows * scale * gain).astype(BF16)
    out = jnp.dot(normed, cols, preferred_element_type=F32).astype(BF16)
    product = out[:, 2 * LANES : 3 * LANES].astype(F32) * out[:, 3 * LANES :].astype(F32)
    pairs = lax.dot_general(normed, kv_rows, (((1,), (1,)), ((), ())), preferred_element_type=F32)
    out_ref[pl.ds(start, count), : 2 * LANES] = out[:, : 2 * LANES]
    out_ref[pl.ds(start, count), 2 * LANES : 3 * LANES] = product.astype(BF16)
    out_ref[pl.ds(start, count), 3 * LANES :] = pairs.astype(BF16)


def take_edge(full_ref, edge_ref, tail):
    total = full_ref.shape[0]
    pair = pl.multiple_of(jnp.where(tail, total - WIN, 0), EDGE)
    lane = lax.broadcasted_iota(jnp.int32, (WIN, LANES), 1)
    keys = full_ref[pl.ds(pair, WIN), 3 * LANES : 4 * LANES].astype(F32)
    values = full_ref[pl.ds(pair, WIN), 4 * LANES :].astype(F32)
    edge_ref[:WIN, :] = jnp.where(lane < HEAD, keys, values).astype(BF16)
    edge = pl.multiple_of(jnp.where(tail, total - EDGE, 0), EDGE)
    edge_ref[WIN:, :] = full_ref[pl.ds(edge, EDGE), 2 * LANES : 3 * LANES]


def near_kernel(*refs):
    *pieces, gain_ref, cols_ref, rows_ref, full_ref, early_ref = refs
    gain, cols, rows = gain_ref[...], cols_ref[...], rows_ref[...]
    place = lax.axis_index("tp")
    chunk = full_ref.shape[0] // 4
    for slot, turn in enumerate((0, 3, 1)):
        start = lax.rem(place + turn, 4) * chunk
        for ref in pieces[2 * slot : 2 * slot + 2]:
            project(ref[...], gain, cols, rows, full_ref, pl.multiple_of(start, EDGE))
            start = start + ref.shape[0]
    take_edge(full_ref, early_ref, place != 1)


def far_kernel(near_ref, top_ref, bottom_ref, gain_ref, cols_ref, rows_ref, full_ref, late_ref):
    gain, cols, rows = gain_ref[...], cols_ref[...], rows_ref[...]
    place = lax.axis_index("tp")
    start = lax.rem(place + 2, 4) * (full_ref.shape[0] // 4)
    for ref in (top_ref, bottom_ref):
        project(ref[...], gain, cols, rows, full_ref, pl.multiple_of(start, EDGE))
        start = start + ref.shape[0]
    take_edge(full_ref, late_ref, place == 1)


def attend(query, keys, values, sink, lowest, highest):
    lane = lax.broadcasted_iota(jnp.int32, (WIN, LANES), 1)
    row = lax.broadcasted_iota(jnp.int32, (2 * WIN, 3 * WIN), 0)
    col = lax.broadcasted_iota(jnp.int32, (2 * WIN, 3 * WIN), 1)
    rel = col - lax.rem(row, WIN)
    allowed = (rel >= 0) & (rel <= 2 * WIN)
    if lowest is not None:
        allowed = allowed & (col >= lowest)
    if highest is not None:
        allowed = allowed & (col < highest)
    zero = jnp.zeros_like(query)
    both = jnp.concatenate([jnp.where(lane < HEAD, query, zero), jnp.where(lane < HEAD, zero, query)], axis=0)
    score = lax.dot_general(both, keys, (((1,), (1,)), ((), ())), preferred_element_type=F32) * HEAD ** (-0.5)
    score = jnp.where(allowed, score, -jnp.inf)
    top = jnp.maximum(jnp.max(score, axis=-1, keepdims=True), sink)
    expo = jnp.exp(score - top)
    denom = jnp.sum(expo, axis=-1, keepdims=True) + jnp.exp(sink - top)
    weights = (expo * (1.0 / denom)).astype(BF16)
    got = jnp.dot(weights, values, preferred_element_type=F32)
    return jnp.where(lane < HEAD, got[:WIN], got[WIN:]).astype(BF16)


def sink_column(sink_ref):
    half = lax.broadcasted_iota(jnp.int32, (2 * WIN, 1), 0) < WIN
    return jnp.where(half, sink_ref[0], sink_ref[1])


def convolve(taps_ref, conv_ref, count):
    return (
        taps_ref[0:1, :] * conv_ref[7 : 7 + count, :]
        + taps_ref[1:2, :] * conv_ref[8 : 8 + count, :]
        + taps_ref[2:3, :] * conv_ref[9 : 9 + count, :]
    )


def inner_kernel(sink_ref, taps_ref, full_ref, out_ref, conv_ref):
    total = full_ref.shape[0]
    conv_ref[0:8, :] = jnp.zeros((8, LANES), F32)
    conv_ref[8 : 8 + total, :] = full_ref[:, 2 * LANES : 3 * LANES].astype(F32)
    conv_ref[8 + total :, :] = jnp.zeros((8, LANES), F32)
    gate = full_ref[:, LANES : 2 * LANES].astype(F32)
    out_ref[:, LANES:] = (gate * convolve(taps_ref, conv_ref, total)).astype(BF16)
    sink = sink_column(sink_ref)
    for at in range(WIN, total - WIN, WIN):
        window = slice(at - WIN, at + 2 * WIN)
        out_ref[at : at + WIN, :LANES] = attend(
            full_ref[at : at + WIN, :LANES],
            full_ref[window, 3 * LANES : 4 * LANES],
            full_ref[window, 4 * LANES :],
            sink,
            None,
            None,
        )


def outer_kernel(sink_ref, taps_ref, full_ref, inner_ref, early_ref, late_ref, out_ref, conv_ref, *, last):
    total = full_ref.shape[0]
    place = lax.axis_index("sp")
    swapped = lax.axis_index("tp") == 1
    early, late = early_ref[...].astype(F32), late_ref[...].astype(F32)
    low, high = jnp.where(swapped, late, early), jnp.where(swapped, early, late)
    lane = lax.broadcasted_iota(jnp.int32, (WIN, LANES), 1)

    def unpack(halo):
        pair = halo[:WIN]
        turned = pltpu.roll(pair, HEAD, 1)
        keys, values = jnp.where(lane < HEAD, pair, turned), jnp.where(lane < HEAD, turned, pair)
        return keys.astype(BF16), values.astype(BF16)

    sink = sink_column(sink_ref)
    for at, halo in ((0, low), (total - WIN, high)):
        first = at == 0
        window = slice(0, 2 * WIN) if first else slice(total - 2 * WIN, total)
        sides = []
        for piece, lanes in zip(unpack(halo), (3, 4)):
            own = full_ref[window, lanes * LANES : (lanes + 1) * LANES]
            sides.append(jnp.concatenate([piece, own] if first else [own, piece], axis=0))
        out_ref[at : at + WIN, :LANES] = attend(
            full_ref[at : at + WIN, :LANES],
            *sides,
            sink,
            jnp.where(place == 0, WIN, 0) if first else None,
            None if first else jnp.where(place == last, 2 * WIN, 3 * WIN),
        )
        if first:
            conv_ref[0:8, :] = halo[WIN + EDGE - 8 :]
            conv_ref[8:32, :] = full_ref[0:32, 2 * LANES : 3 * LANES].astype(F32)[:24]
        else:
            conv_ref[0:24, :] = full_ref[total - 32 :, 2 * LANES : 3 * LANES].astype(F32)[8:]
            conv_ref[24:32, :] = halo[WIN : WIN + 8]
        rows = slice(0, EDGE) if first else slice(total - EDGE, total)
        gate = full_ref[rows, LANES : 2 * LANES].astype(F32)
        out_ref[rows, LANES:] = (gate * convolve(taps_ref, conv_ref, EDGE)).astype(BF16)


def out_kernel(parts_ref, weight_ref, out_ref, done_ref, sems):
    count = parts_ref.shape[0]
    joined = jnp.concatenate(
        [parts_ref[i, :, :LANES] for i in range(count)] + [parts_ref[i, :, LANES:] for i in range(count)], axis=1
    )
    steps, _, step = done_ref.shape
    copies = []
    for i in range(steps):
        columns = pl.ds(i * step, step)
        done_ref[i] = jnp.dot(joined, weight_ref[:, columns], preferred_element_type=F32).astype(BF16)
        copies.append(pltpu.make_async_copy(done_ref.at[i], out_ref.at[:, columns], sems.at[i]))
        copies[-1].start()
    for copy in copies:
        copy.wait()


def body(
    tokens,
    norm_gain,
    query_weight,
    key_weight,
    value_weight,
    sink_logit,
    conv_gate_weight,
    conv_pre_weight,
    conv_input_weight,
    conv_taps,
    out_weight,
):
    chunk, width = tokens.shape
    total = 4 * chunk

    def local(kernel, shapes, count, **more):
        return pl.pallas_call(
            kernel,
            out_shape=tuple(pltpu.VMEM(shape, dtype) for shape, dtype in shapes),
            in_specs=[VMEM] * count,
            out_specs=(VMEM,) * len(shapes),
            compiler_params=params(16),
            **more,
        )

    def in_hbm(*arrays):
        return tuple(pltpu.with_memory_space_constraint(array, pltpu.HBM) for array in arrays)

    def loader(kernel, shapes, count):
        return pl.pallas_call(
            kernel,
            out_shape=tuple(pltpu.VMEM(shape, dtype) for shape, dtype in shapes),
            in_specs=[pl.BlockSpec(memory_space=pltpu.HBM)] * count,
            out_specs=(VMEM,) * len(shapes),
            scratch_shapes=[pltpu.SemaphoreType.DMA((9,))],
            compiler_params=params(16),
        )

    forward = [(i, (i + 1) % 4) for i in range(4)]
    backward = [(i, (i + 3) % 4) for i in range(4)]
    lead = chunk // 2 + EDGE
    top, bottom = loader(split_kernel, (((lead, width), BF16), ((chunk - lead, width), BF16)), 1)(*in_hbm(tokens))

    before_top = lax.ppermute(top, "tp", forward)
    after_bottom = lax.ppermute(bottom, "tp", backward)
    before_bottom = lax.ppermute(bottom, "tp", forward)
    after_top = lax.ppermute(top, "tp", backward)
    far_top = lax.ppermute(before_top, "tp", forward)
    far_bottom = lax.ppermute(after_bottom, "tp", backward)

    packed = loader(pack_kernel, (((width, 4 * LANES), BF16), ((2 * LANES, width), BF16), ((1, width), F32)), 7)(
        *in_hbm(
            query_weight,
            key_weight.T,
            value_weight.T,
            conv_gate_weight,
            conv_pre_weight,
            conv_input_weight,
            norm_gain.reshape(1, width),
        )
    )
    cols, rows, gain = packed
    weights = (gain, cols, rows)
    full_shape = ((total, 5 * LANES), BF16)
    edge_shape = ((WIN + EDGE, LANES), BF16)
    full, early = local(near_kernel, (full_shape, edge_shape), 9)(
        *near_memory(top, bottom, before_top, before_bottom, after_top, after_bottom, *weights)
    )
    count = lax.axis_size("sp")
    ups = {x: [(4 * i + x, 4 * i + 4 + x) for i in range(count - 1)] for x in range(4)}
    downs = {x: [(j, i) for i, j in pairs] for x, pairs in ups.items()}
    early = lax.ppermute(early, ("sp", "tp"), ups[0] + downs[1] + ups[2] + ups[3])
    full, late = local(far_kernel, (full_shape, edge_shape), 6, input_output_aliases={0: 0})(
        *near_memory(full, far_top, far_bottom, *weights)
    )
    late = lax.ppermute(late, ("sp", "tp"), downs[0] + ups[1] + downs[2] + downs[3])

    def outer(*refs):
        outer_kernel(*refs, last=count - 1)

    def mixer(kernel, inputs, rows, **more):
        return pl.pallas_call(
            kernel,
            out_shape=pltpu.VMEM((total, 2 * LANES), BF16),
            in_specs=[SMEM] + [VMEM] * inputs,
            out_specs=VMEM,
            scratch_shapes=[pltpu.VMEM((rows, LANES), F32)],
            compiler_params=params(16),
            **more,
        )

    (taps,) = near_memory(conv_taps)
    inner = mixer(inner_kernel, 2, total + 16)(sink_logit, taps, *near_memory(full))
    mixed = mixer(outer, 5, 32, input_output_aliases={3: 0})(sink_logit, taps, *near_memory(full, inner, early, late))
    parts = lax.all_to_all(mixed.reshape(4, chunk, 2 * LANES), "tp", split_axis=0, concat_axis=0, tiled=True)
    step = 512
    steps = out_weight.shape[1] // step
    return pl.pallas_call(
        out_kernel,
        name="project_out",
        out_shape=jax.ShapeDtypeStruct((chunk, out_weight.shape[1]), BF16),
        in_specs=[VMEM] * 2,
        out_specs=pl.BlockSpec(memory_space=pltpu.HBM),
        scratch_shapes=[pltpu.VMEM((steps, chunk, step), BF16), pltpu.SemaphoreType.DMA((steps,))],
        compiler_params=params(16),
    )(*near_memory(parts, out_weight))


def solution(mesh):
    placed = (
        P(("sp", "tp"), None),
        P(),
        P(None, "tp"),
        P(None, "tp"),
        P(None, "tp"),
        P("tp"),
        P(None, "tp"),
        P(None, "tp"),
        P(None, "tp"),
        P(None, "tp"),
        P(),
    )

    return jax.shard_map(body, mesh=mesh, in_specs=placed, out_specs=P(("sp", "tp"), None), check_vma=False)
```

time: 70.5 us -> 73.1 us (1.037)
  waiting for transfers between devices: 0.85 us -> 8.68 us
  local copies, waits for them, and re-layouts: 6.76 us -> 0.01 us
  Pallas kernels: 13.3 us -> 14.9 us
    ppermute x1, waiting for transfers between devices: 0.01 us -> 8.11 us  [body(): before_bottom = lax.ppermute(bottom, 'tp', forward)]
    unnamed x20 -> x6, local copies, waits for them, and re-layouts: 6.76 us -> 0.01 us
    ppermute x1, starting transfers between devices: 1.92 us -> 5.17 us  [body(): far_top = lax.ppermute(before_top, 'tp', forward)]
    pallas_call x5 -> x6, Pallas kernels: 10.6 us -> 13.2 us  [the longest x1 4.27 us: body(): local(near_kernel, (full_shape, edge_shape), 9)]
    ppermute x2, starting transfers between devices: 18.4 us -> 16.1 us  [the longest x1 8.69 us: body(): lax.ppermute(early, ('sp', 'tp'), ups[0] + downs[1] + ups[2] + ups[3])]
    ppermute x1, starting transfers between devices: 4.57 us -> 2.38 us  [body(): far_bottom = lax.ppermute(after_bottom, 'tp', backward)]
    ppermute x1, starting transfers between devices: 2.09 us -> 4.11 us  [body(): before_bottom = lax.ppermute(bottom, 'tp', forward)]
    pallas_call x1, Pallas kernels: 2.78 us -> 1.74 us  [body(): pl.pallas_call(out_kernel, name='project_out', out_shape=jax.ShapeDtypeSt...]
  transfers between devices with their start and end apart: 8 -> 8, of which waited for: 1 -> 2; matrix products, arithmetic and copies ran while one was open for 0% -> 0% of each run, Pallas kernels for 6% -> 14%
where the time goes in v2:
time: 73.1 us; the launch traced here: 72.7 us
  starting transfers between devices  38.3 us (52%)
  Pallas kernels  14.9 us (20%)
  blocking collectives  10.7 us (15%)
  waiting for transfers between devices  8.68 us (12%)
    all_to_all x1, blocking collectives, body(): lax.all_to_all(mixed.reshape(4, chunk, 2 * LANES), 'tp', split_axis=0, co...  10.7 us
    ppermute x1, starting transfers between devices, body(): lax.ppermute(early, ('sp', 'tp'), ups[0] + downs[1] + ups[2] + ups[3])  8.69 us
    ppermute x1, waiting for transfers between devices, body(): before_bottom = lax.ppermute(bottom, 'tp', forward)  8.11 us
    ppermute x1, starting transfers between devices, body(): lax.ppermute(late, ('sp', 'tp'), downs[0] + ups[1] + downs[2] + downs[3])  7.43 us
    ppermute x1, starting transfers between devices, body(): far_top = lax.ppermute(before_top, 'tp', forward)  5.17 us
    pallas_call x1, Pallas kernels, body(): local(near_kernel, (full_shape, edge_shape), 9)  4.27 us
    ppermute x1, starting transfers between devices, body(): before_bottom = lax.ppermute(bottom, 'tp', forward)  4.11 us
    ppermute x1, starting transfers between devices, body(): before_top = lax.ppermute(top, 'tp', forward)  3.94 us
  transfers between devices with their start and end apart: 8, of which 2 were waited for; matrix products, arithmetic and copies ran while one was open for 0% of the time, Pallas kernels for 14%

profile of v2, /device:TPU:1, one launch (start us, length us, event | category | flops | bytes accessed | tf_op | source)
XLA Modules:
  0.0 72.7 jit_solution(9459090259648541566)
XLA Ops:
  0.0 1.2 %shard_map.109 = (bf16[112,2048]{1,0:T(8,128)(2,1)S(1)}, bf16[80,2048]{1,0:T(8,128)(2,1)S(1)}) custom-call(bf16[192,2048]{1,0:T(8,128)(2,1)} %tokens_ref.1), custom_call_target="tpu_custom_call" | custom-call | tf_op jit(solution)/shard_map/pallas_call | solution.py:257
  1.2 3.9 %collective-permute-start = (bf16[112,2048]{1,0:T(8,128)(2,1)S(1)}, bf16[112,2048]{1,0:T(8,128)(2,1)S(1)}, u32[]{:S(2)}, u32[]{:S(2)}) collective-permute-start(bf16[112,2048]{1,0:T(8,128)(2,1)S(1)} %get-tuple-element.14.refs_0_), channel_id=1, source_target_pairs={{0,1},{1,2},{2,3},{3,0},{4,5},{5,6},{6,7},{7,4},{8,9},{9,10},{10,1... | collective-permute-start | bytes 1376264 | tf_op jit(solution)/shard_map/ppermute | solution.py:259
  5.1 3.2 %collective-permute-start.3 = (bf16[80,2048]{1,0:T(8,128)(2,1)S(1)}, bf16[80,2048]{1,0:T(8,128)(2,1)S(1)}, u32[]{:S(2)}, u32[]{:S(2)}) collective-permute-start(bf16[80,2048]{1,0:T(8,128)(2,1)S(1)} %get-tuple-element.15.refs_1_), channel_id=1, source_target_pairs={{0,3},{1,0},{2,1},{3,2},{4,7},{5,4},{6,5},{7,6},{8,11},{9,8},{10,9... | collective-permute-start | bytes 983048 | tf_op jit(solution)/shard_map/ppermute | solution.py:260
  8.3 3.4 %collective-permute-start.2 = (bf16[112,2048]{1,0:T(8,128)(2,1)S(1)}, bf16[112,2048]{1,0:T(8,128)(2,1)S(1)}, u32[]{:S(2)}, u32[]{:S(2)}) collective-permute-start(bf16[112,2048]{1,0:T(8,128)(2,1)S(1)} %get-tuple-element.14.refs_0_), channel_id=1, source_target_pairs={{0,3},{1,0},{2,1},{3,2},{4,7},{5,4},{6,5},{7,6},{8,11},{9,8},{10,9... | collective-permute-start | bytes 1376264 | tf_op jit(solution)/shard_map/ppermute | solution.py:262
  11.7 0.6 collective-permute-done.refs_2_
  12.3 5.2 %collective-permute-start.4 = (bf16[112,2048]{1,0:T(8,128)(2,1)S(1)}, bf16[112,2048]{1,0:T(8,128)(2,1)S(1)}, u32[]{:S(2)}, u32[]{:S(2)}) collective-permute-start(bf16[112,2048]{1,0:T(8,128)(2,1)S(1)} %collective-permute-done.refs_2_), channel_id=1, source_target_pairs={{0,1},{1,2},{2,3},{3,0},{4,5},{5,6},{6,7},{7,4},{8,9},{9,10},{10,1... | collective-permute-start | bytes 1376264 | tf_op jit(solution)/shard_map/ppermute | solution.py:263
  17.4 4.1 %collective-permute-start.1 = (bf16[80,2048]{1,0:T(8,128)(2,1)S(1)}, bf16[80,2048]{1,0:T(8,128)(2,1)S(1)}, u32[]{:S(2)}, u32[]{:S(2)}) collective-permute-start(bf16[80,2048]{1,0:T(8,128)(2,1)S(1)} %get-tuple-element.15.refs_1_), channel_id=1, source_target_pairs={{0,1},{1,2},{2,3},{3,0},{4,5},{5,6},{6,7},{7,4},{8,9},{9,10},{10,1... | collective-permute-start | bytes 983048 | tf_op jit(solution)/shard_map/ppermute | solution.py:261
  21.6 0.0 collective-permute-done.3.refs_5_
  21.6 2.4 %collective-permute-start.5 = (bf16[80,2048]{1,0:T(8,128)(2,1)S(1)}, bf16[80,2048]{1,0:T(8,128)(2,1)S(1)}, u32[]{:S(2)}, u32[]{:S(2)}) collective-permute-start(bf16[80,2048]{1,0:T(8,128)(2,1)S(1)} %collective-permute-done.3.refs_5_), channel_id=1, source_target_pairs={{0,3},{1,0},{2,1},{3,2},{4,7},{5,4},{6,5},{7,6},{8,11},{9,8},{10,9... | collective-permute-start | bytes 983048 | tf_op jit(solution)/shard_map/ppermute | solution.py:264
  24.0 1.9 %shard_map.110 = (bf16[2048,512]{1,0:T(8,128)(2,1)S(1)}, bf16[256,2048]{1,0:T(8,128)(2,1)S(1)}, f32[1,2048]{1,0:T(1,128)S(1)}) custom-call(bf16[2048,128]{1,0:T(8,128)(2,1)} %q_ref.1, bf16[64,2048]{1,0:T(8,128)(2,1)} %bitcast.5, bf16[64,2048]{1,0:T(8,128)(2,1)} %bitcast.6, bf16[2048,128]{1,0:T(8,128)(2,1)} %gate_ref.1, bf16[2048,128]{1,0:T(8,128)(2,1)} %pre_ref.1, ...), custom_call_target="tpu_custom_call" | custom-call | tf_op jit(solution)/shard_map/pallas_call | solution.py:266
  25.9 8.1 %collective-permute-done.1.refs_3_ = bf16[80,2048]{1,0:T(8,128)(2,1)S(1)} collective-permute-done((bf16[80,2048]{1,0:T(8,128)(2,1)S(1)}, bf16[80,2048]{1,0:T(8,128)(2,1)S(1)}, u32[]{:S(2)}, u32[]{:S(2)}) %collective-permute-start.1) | collective-permute-done | bytes 327712 | tf_op jit(solution)/shard_map/ppermute | solution.py:261
  34.0 0.0 collective-permute-done.2.refs_4_
  34.0 0.0 copy-start.1
  34.0 0.0 copy-start.2
  34.0 4.3 %shard_map.111 = (bf16[768,640]{1,0:T(8,128)(2,1)S(1)}, bf16[144,128]{1,0:T(8,128)(2,1)S(1)}) custom-call(bf16[112,2048]{1,0:T(8,128)(2,1)S(1)} %get-tuple-element.14.refs_0_, bf16[80,2048]{1,0:T(8,128)(2,1)S(1)} %get-tuple-element.15.refs_1_, bf16[112,2048]{1,0:T(8,128)(2,1)S(1)} %collective-permute-done.refs_2_, ...), custom_call_target="tpu_custom_call" | custom-call | tf_op jit(solution)/shard_map/pallas_call | solution.py:281
  38.3 8.7 %collective-permute-start.6 = (bf16[144,128]{1,0:T(8,128)(2,1)S(1)}, bf16[144,128]{1,0:T(8,128)(2,1)S(1)}, u32[]{:S(2)}, u32[]{:S(2)}) collective-permute-start(bf16[144,128]{1,0:T(8,128)(2,1)S(1)} %get-tuple-element.21), channel_id=1, source_target_pairs={{0,4},{4,8},{8,12},{12,16},{16,20},{20,24},{24,28},{28,32},{32,36}... | collective-permute-start | bytes 110600 | tf_op jit(solution)/shard_map/ppermute | solution.py:287
  47.0 0.0 collective-permute-done.5.bottom_ref
  47.0 0.0 collective-permute-done.4.top_ref
  47.0 0.0 copy-start
  47.0 1.6 %shard_map.112 = (bf16[768,640]{1,0:T(8,128)(2,1)S(1)}, bf16[144,128]{1,0:T(8,128)(2,1)S(1)}) custom-call(bf16[768,640]{1,0:T(8,128)(2,1)S(1)} %get-tuple-element.19.near_ref, bf16[112,2048]{1,0:T(8,128)(2,1)S(1)} %collective-permute-done.4.top_ref, bf16[80,2048]{1,0:T(8,128)(2,1)S(1)} %collective-permute-done.5.bottom_ref, ...), custom_call_target="tpu_custom_call", output_to_operand_aliasing={{0}: (0, {})} | custom-call | tf_op jit(solution)/shard_map/pallas_call | solution.py:288
  48.6 7.4 %collective-permute-start.7 = (bf16[144,128]{1,0:T(8,128)(2,1)S(1)}, bf16[144,128]{1,0:T(8,128)(2,1)S(1)}, u32[]{:S(2)}, u32[]{:S(2)}) collective-permute-start(bf16[144,128]{1,0:T(8,128)(2,1)S(1)} %get-tuple-element.22), channel_id=1, source_target_pairs={{4,0},{8,4},{12,8},{16,12},{20,16},{24,20},{28,24},{32,28},{36,32}... | collective-permute-start | bytes 110600 | tf_op jit(solution)/shard_map/ppermute | solution.py:291
  56.1 0.0 copy-done.1
  56.1 0.0 copy-done.2
  56.1 2.6 %shard_map.113.refs_3_ = bf16[768,256]{1,0:T(8,128)(2,1)S(1)} custom-call(f32[2]{0:T(128)S(1)} %copy-done.2, f32[3,128]{1,0:T(4,128)S(1)} %copy-done.1, bf16[768,640]{1,0:T(8,128)(2,1)S(1)} %get-tuple-element.20.full_ref.refs_2_), custom_call_target="tpu_custom_call" | custom-call | tf_op jit(solution)/shard_map/pallas_call | solution.py:308
  58.6 0.0 collective-permute-done.6.refs_4_
  58.7 0.0 collective-permute-done.7.refs_5_
  58.7 1.6 %shard_map.114 = bf16[768,256]{1,0:T(8,128)(2,1)S(1)} custom-call(f32[2]{0:T(128)S(1)} %copy-done.2, f32[3,128]{1,0:T(4,128)S(1)} %copy-done.1, bf16[768,640]{1,0:T(8,128)(2,1)S(1)} %get-tuple-element.20.full_ref.refs_2_, bf16[768,256]{1,0:T(8,128)(2,1)S(1)} %shard_map.113.refs_3_, ...), custom_call_target="tpu_custom_call", output_to_operand_aliasing={{}: (3, {})} | custom-call | tf_op jit(solution)/shard_map/pallas_call | solution.py:309
  60.3 10.7 %all_to_all.5.parts_ref = bf16[4,192,256]{2,1,0:T(8,128)(2,1)S(1)} all-to-all(bf16[4,192,256]{2,1,0:T(8,128)(2,1)S(1)} %bitcast.4), channel_id=1, replica_groups=mesh['sp'=256,'tp'=4] {'tp'}, dimensions={0} | all-to-all | bytes 786432 | tf_op jit(solution)/shard_map/all_to_all | solution.py:310
  71.0 0.0 copy-done
  71.0 1.7 %project_out.1 = bf16[192,2048]{1,0:T(8,128)(2,1)} custom-call(bf16[4,192,256]{2,1,0:T(8,128)(2,1)S(1)} %all_to_all.5.parts_ref, bf16[1024,2048]{1,0:T(8,128)(2,1)S(1)} %copy-done), custom_call_target="tpu_custom_call" | custom-call | tf_op jit(solution)/shard_map/project_out/pallas_call | solution.py:313
Async XLA Ops:
  1.2 11.1 %collective-permute-start = (bf16[112,2048]{1,0:T(8,128)(2,1)S(1)}, bf16[112,2048]{1,0:T(8,128)(2,1)S(1)}, u32[]{:S(2)}, u32[]{:S(2)}) collective-permute-start(bf16[112,2048]{1,0:T(8,128)(2,1)S(1)} %get-tuple-element.14.refs_0_), channel_id=1, source_target_pairs={{0,1},{1,2},{2,3},{3,0},{4,5},{5,6},{6,7},{7,4},{8,9},{9,10},{10,1... | collective-permute-start | bytes 1376264 | tf_op jit(solution)/shard_map/ppermute | solution.py:259
  5.1 16.4 %collective-permute-start.3 = (bf16[80,2048]{1,0:T(8,128)(2,1)S(1)}, bf16[80,2048]{1,0:T(8,128)(2,1)S(1)}, u32[]{:S(2)}, u32[]{:S(2)}) collective-permute-start(bf16[80,2048]{1,0:T(8,128)(2,1)S(1)} %get-tuple-element.15.refs_1_), channel_id=1, source_target_pairs={{0,3},{1,0},{2,1},{3,2},{4,7},{5,4},{6,5},{7,6},{8,11},{9,8},{10,9... | collective-permute-start | bytes 983048 | tf_op jit(solution)/shard_map/ppermute | solution.py:260
  8.3 25.6 %collective-permute-start.2 = (bf16[112,2048]{1,0:T(8,128)(2,1)S(1)}, bf16[112,2048]{1,0:T(8,128)(2,1)S(1)}, u32[]{:S(2)}, u32[]{:S(2)}) collective-permute-start(bf16[112,2048]{1,0:T(8,128)(2,1)S(1)} %get-tuple-element.14.refs_0_), channel_id=1, source_target_pairs={{0,3},{1,0},{2,1},{3,2},{4,7},{5,4},{6,5},{7,6},{8,11},{9,8},{10,9... | collective-permute-start | bytes 1376264 | tf_op jit(solution)/shard_map/ppermute | solution.py:262
  12.3 34.7 %collective-permute-start.4 = (bf16[112,2048]{1,0:T(8,128)(2,1)S(1)}, bf16[112,2048]{1,0:T(8,128)(2,1)S(1)}, u32[]{:S(2)}, u32[]{:S(2)}) collective-permute-start(bf16[112,2048]{1,0:T(8,128)(2,1)S(1)} %collective-permute-done.refs_2_), channel_id=1, source_target_pairs={{0,1},{1,2},{2,3},{3,0},{4,5},{5,6},{6,7},{7,4},{8,9},{9,10},{10,1... | collective-permute-start | bytes 1376264 | tf_op jit(solution)/shard_map/ppermute | solution.py:263
  17.4 16.5 %collective-permute-start.1 = (bf16[80,2048]{1,0:T(8,128)(2,1)S(1)}, bf16[80,2048]{1,0:T(8,128)(2,1)S(1)}, u32[]{:S(2)}, u32[]{:S(2)}) collective-permute-start(bf16[80,2048]{1,0:T(8,128)(2,1)S(1)} %get-tuple-element.15.refs_1_), channel_id=1, source_target_pairs={{0,1},{1,2},{2,3},{3,0},{4,5},{5,6},{6,7},{7,4},{8,9},{9,10},{10,1... | collective-permute-start | bytes 983048 | tf_op jit(solution)/shard_map/ppermute | solution.py:261
  21.6 25.4 %collective-permute-start.5 = (bf16[80,2048]{1,0:T(8,128)(2,1)S(1)}, bf16[80,2048]{1,0:T(8,128)(2,1)S(1)}, u32[]{:S(2)}, u32[]{:S(2)}) collective-permute-start(bf16[80,2048]{1,0:T(8,128)(2,1)S(1)} %collective-permute-done.3.refs_5_), channel_id=1, source_target_pairs={{0,3},{1,0},{2,1},{3,2},{4,7},{5,4},{6,5},{7,6},{8,11},{9,8},{10,9... | collective-permute-start | bytes 983048 | tf_op jit(solution)/shard_map/ppermute | solution.py:264
  34.0 22.1 %copy-start.1 = (f32[3,128]{1,0:T(4,128)S(1)}, f32[3,128]{1,0:T(4,128)}, u32[]{:S(2)}) copy-start(f32[3,128]{1,0:T(4,128)} %refs_1_.1) | copy-start | bytes 4612
  34.0 22.1 %copy-start.2 = (f32[2]{0:T(128)S(1)}, f32[2]{0:T(128)}, u32[]{:S(2)}) copy-start(f32[2]{0:T(128)} %refs_0_.1) | copy-start | bytes 28
  38.3 20.4 %collective-permute-start.6 = (bf16[144,128]{1,0:T(8,128)(2,1)S(1)}, bf16[144,128]{1,0:T(8,128)(2,1)S(1)}, u32[]{:S(2)}, u32[]{:S(2)}) collective-permute-start(bf16[144,128]{1,0:T(8,128)(2,1)S(1)} %get-tuple-element.21), channel_id=1, source_target_pairs={{0,4},{4,8},{8,12},{12,16},{16,20},{20,24},{24,28},{28,32},{32,36}... | collective-permute-start | bytes 110600 | tf_op jit(solution)/shard_map/ppermute | solution.py:287
  47.0 24.0 %copy-start = (bf16[1024,2048]{1,0:T(8,128)(2,1)S(1)}, bf16[1024,2048]{1,0:T(8,128)(2,1)}, u32[]{:S(2)}) copy-start(bf16[1024,2048]{1,0:T(8,128)(2,1)} %weight_ref.1) | copy-start | bytes 12582916
  48.6 10.0 %collective-permute-start.7 = (bf16[144,128]{1,0:T(8,128)(2,1)S(1)}, bf16[144,128]{1,0:T(8,128)(2,1)S(1)}, u32[]{:S(2)}, u32[]{:S(2)}) collective-permute-start(bf16[144,128]{1,0:T(8,128)(2,1)S(1)} %get-tuple-element.22), channel_id=1, source_target_pairs={{4,0},{8,4},{12,8},{16,12},{20,16},{24,20},{28,24},{32,28},{36,32}... | collective-permute-start | bytes 110600 | tf_op jit(solution)/shard_map/ppermute | solution.py:291

commit v3 on v2

--- a/solution.py
+++ b/solution.py
@@ -83,8 +83,8 @@
     gain, cols, rows = gain_ref[...], cols_ref[...], rows_ref[...]
     place = lax.axis_index("tp")
     chunk = full_ref.shape[0] // 4
-    for slot, turn in enumerate((0, 3, 1)):
-        start = lax.rem(place + turn, 4) * chunk
+    for slot, turn in enumerate((0, 1, 3)):
+        start = (place ^ turn) * chunk
         for ref in pieces[2 * slot : 2 * slot + 2]:
             project(ref[...], gain, cols, rows, full_ref, pl.multiple_of(start, EDGE))
             start = start + ref.shape[0]
@@ -94,7 +94,7 @@
 def far_kernel(near_ref, top_ref, bottom_ref, gain_ref, cols_ref, rows_ref, full_ref, late_ref):
     gain, cols, rows = gain_ref[...], cols_ref[...], rows_ref[...]
     place = lax.axis_index("tp")
-    start = lax.rem(place + 2, 4) * (full_ref.shape[0] // 4)
+    start = (place ^ 2) * (full_ref.shape[0] // 4)
     for ref in (top_ref, bottom_ref):
         project(ref[...], gain, cols, rows, full_ref, pl.multiple_of(start, EDGE))
         start = start + ref.shape[0]
@@ -251,17 +251,18 @@
             compiler_params=params(16),
         )
 
-    forward = [(i, (i + 1) % 4) for i in range(4)]
-    backward = [(i, (i + 3) % 4) for i in range(4)]
-    lead = chunk // 2 + EDGE
+    lead = chunk // 2 - EDGE
     top, bottom = loader(split_kernel, (((lead, width), BF16), ((chunk - lead, width), BF16)), 1)(*in_hbm(tokens))
 
-    before_top = lax.ppermute(top, "tp", forward)
-    after_bottom = lax.ppermute(bottom, "tp", backward)
-    before_bottom = lax.ppermute(bottom, "tp", forward)
-    after_top = lax.ppermute(top, "tp", backward)
-    far_top = lax.ppermute(before_top, "tp", forward)
-    far_bottom = lax.ppermute(after_bottom, "tp", backward)
+    def swap(block, turn):
+        return lax.ppermute(block, "tp", [(i, i ^ turn) for i in range(4)])
+
+    a_top = swap(top, 1)
+    b_bottom = swap(bottom, 3)
+    a_bottom = swap(bottom, 1)
+    b_top = swap(top, 3)
+    far_top = swap(a_top, 3)
+    far_bottom = swap(b_bottom, 1)
 
     packed = loader(pack_kernel, (((width, 4 * LANES), BF16), ((2 * LANES, width), BF16), ((1, width), F32)), 7)(
         *in_hbm(
@@ -279,7 +280,7 @@
     full_shape = ((total, 5 * LANES), BF16)
     edge_shape = ((WIN + EDGE, LANES), BF16)
     full, early = local(near_kernel, (full_shape, edge_shape), 9)(
-        *near_memory(top, bottom, before_top, before_bottom, after_top, after_bottom, *weights)
+        *near_memory(top, bottom, a_top, a_bottom, b_top, b_bottom, *weights)
     )
     count = lax.axis_size("sp")
     ups = {x: [(4 * i + x, 4 * i + 4 + x) for i in range(count - 1)] for x in range(4)}

time: 73.1 us -> 66.3 us (0.907)
  waiting for transfers between devices: 8.68 us -> 3.43 us
  blocking collectives: 10.7 us -> 9.67 us
    ppermute x6, waiting for transfers between devices: 8.67 us -> 3.42 us  [swap(): return lax.ppermute(block, 'tp', [(i, i ^ turn) for i in range(4)])]
    ppermute x1, starting transfers between devices: 8.69 us -> 7.29 us  [body(): lax.ppermute(early, ('sp', 'tp'), ups[0] + downs[1] + ups[2] + ups[3])]
    all_to_all x1, blocking collectives: 10.7 us -> 9.67 us  [body(): lax.all_to_all(mixed.reshape(4, chunk, 2 * LANES), 'tp', split_axis=0, co...]
    ppermute x6, starting transfers between devices: 22.1 us -> 23.1 us  [swap(): return lax.ppermute(block, 'tp', [(i, i ^ turn) for i in range(4)])]
  transfers between devices with their start and end apart: 8 -> 8, of which waited for: 2 -> 2; matrix products, arithmetic and copies ran while one was open for 0% -> 0% of each run, Pallas kernels for 14% -> 15%
where the time goes in v3:
time: 66.3 us; the launch traced here: 65.9 us
  starting transfers between devices  37.9 us (57%)
  Pallas kernels  14.7 us (22%)
  blocking collectives  9.67 us (15%)
  waiting for transfers between devices  3.43 us (5%)
    ppermute x6, starting transfers between devices, swap(): return lax.ppermute(block, 'tp', [(i, i ^ turn) for i in range(4)])  23.1 us
    all_to_all x1, blocking collectives, body(): lax.all_to_all(mixed.reshape(4, chunk, 2 * LANES), 'tp', split_axis=0, co...  9.67 us
    ppermute x1, starting transfers between devices, body(): lax.ppermute(late, ('sp', 'tp'), downs[0] + ups[1] + downs[2] + downs[3])  7.44 us
    ppermute x1, starting transfers between devices, body(): lax.ppermute(early, ('sp', 'tp'), ups[0] + downs[1] + ups[2] + ups[3])  7.29 us
    pallas_call x1, Pallas kernels, body(): local(near_kernel, (full_shape, edge_shape), 9)  4.16 us
    ppermute x6, waiting for transfers between devices, swap(): return lax.ppermute(block, 'tp', [(i, i ^ turn) for i in range(4)])  3.42 us
    pallas_call x1, Pallas kernels, body(): mixer(inner_kernel, 2, total + 16)(sink_logit, taps, *near_memory(full))  2.56 us
    pallas_call x1, Pallas kernels, body(): loader(pack_kernel, (((width, 4 * LANES), BF16), ((2 * LANES, width), BF1...  1.9 us
  transfers between devices with their start and end apart: 8, of which 2 were waited for; matrix products, arithmetic and copies ran while one was open for 0% of the time, Pallas kernels for 15%

profile of v3, /device:TPU:1, one launch (start us, length us, event | category | flops | bytes accessed | tf_op | source)
XLA Modules:
  0.0 65.9 jit_solution(15554281335770080681)
XLA Ops:
  0.0 1.2 %shard_map.109 = (bf16[80,2048]{1,0:T(8,128)(2,1)S(1)}, bf16[112,2048]{1,0:T(8,128)(2,1)S(1)}) custom-call(bf16[192,2048]{1,0:T(8,128)(2,1)} %tokens_ref.1), custom_call_target="tpu_custom_call" | custom-call | tf_op jit(solution)/shard_map/pallas_call | solution.py:255
  1.2 5.2 %collective-permute-start.3 = (bf16[112,2048]{1,0:T(8,128)(2,1)S(1)}, bf16[112,2048]{1,0:T(8,128)(2,1)S(1)}, u32[]{:S(2)}, u32[]{:S(2)}) collective-permute-start(bf16[112,2048]{1,0:T(8,128)(2,1)S(1)} %get-tuple-element.15.refs_1_), channel_id=1, source_target_pairs={{0,3},{1,2},{2,1},{3,0},{4,7},{5,6},{6,5},{7,4},{8,11},{9,10},{10,... | collective-permute-start | bytes 1376264 | tf_op jit(solution)/shard_map/ppermute | solution.py:258
  6.4 1.9 %collective-permute-start = (bf16[80,2048]{1,0:T(8,128)(2,1)S(1)}, bf16[80,2048]{1,0:T(8,128)(2,1)S(1)}, u32[]{:S(2)}, u32[]{:S(2)}) collective-permute-start(bf16[80,2048]{1,0:T(8,128)(2,1)S(1)} %get-tuple-element.14.refs_0_), channel_id=1, source_target_pairs={{0,1},{1,0},{2,3},{3,2},{4,5},{5,4},{6,7},{7,6},{8,9},{9,8},{10,11... | collective-permute-start | bytes 983048 | tf_op jit(solution)/shard_map/ppermute | solution.py:258
  8.3 3.4 %collective-permute-start.1 = (bf16[112,2048]{1,0:T(8,128)(2,1)S(1)}, bf16[112,2048]{1,0:T(8,128)(2,1)S(1)}, u32[]{:S(2)}, u32[]{:S(2)}) collective-permute-start(bf16[112,2048]{1,0:T(8,128)(2,1)S(1)} %get-tuple-element.15.refs_1_), channel_id=1, source_target_pairs={{0,1},{1,0},{2,3},{3,2},{4,5},{5,4},{6,7},{7,6},{8,9},{9,8},{10,11... | collective-permute-start | bytes 1376264 | tf_op jit(solution)/shard_map/ppermute | solution.py:258
  11.7 0.6 collective-permute-done.3.refs_5_
  12.3 6.2 %collective-permute-start.5 = (bf16[112,2048]{1,0:T(8,128)(2,1)S(1)}, bf16[112,2048]{1,0:T(8,128)(2,1)S(1)}, u32[]{:S(2)}, u32[]{:S(2)}) collective-permute-start(bf16[112,2048]{1,0:T(8,128)(2,1)S(1)} %collective-permute-done.3.refs_5_), channel_id=1, source_target_pairs={{0,1},{1,0},{2,3},{3,2},{4,5},{5,4},{6,7},{7,6},{8,9},{9,8},{10,11... | collective-permute-start | bytes 1376264 | tf_op jit(solution)/shard_map/ppermute | solution.py:258
  18.4 3.7 %collective-permute-start.2 = (bf16[80,2048]{1,0:T(8,128)(2,1)S(1)}, bf16[80,2048]{1,0:T(8,128)(2,1)S(1)}, u32[]{:S(2)}, u32[]{:S(2)}) collective-permute-start(bf16[80,2048]{1,0:T(8,128)(2,1)S(1)} %get-tuple-element.14.refs_0_), channel_id=1, source_target_pairs={{0,3},{1,2},{2,1},{3,0},{4,7},{5,6},{6,5},{7,4},{8,11},{9,10},{10,... | collective-permute-start | bytes 983048 | tf_op jit(solution)/shard_map/ppermute | solution.py:258
  22.2 0.0 collective-permute-done.refs_2_
  22.2 2.8 %collective-permute-start.4 = (bf16[80,2048]{1,0:T(8,128)(2,1)S(1)}, bf16[80,2048]{1,0:T(8,128)(2,1)S(1)}, u32[]{:S(2)}, u32[]{:S(2)}) collective-permute-start(bf16[80,2048]{1,0:T(8,128)(2,1)S(1)} %collective-permute-done.refs_2_), channel_id=1, source_target_pairs={{0,3},{1,2},{2,1},{3,0},{4,7},{5,6},{6,5},{7,4},{8,11},{9,10},{10,... | collective-permute-start | bytes 983048 | tf_op jit(solution)/shard_map/ppermute | solution.py:258
  25.0 1.9 %shard_map.110 = (bf16[2048,512]{1,0:T(8,128)(2,1)S(1)}, bf16[256,2048]{1,0:T(8,128)(2,1)S(1)}, f32[1,2048]{1,0:T(1,128)S(1)}) custom-call(bf16[2048,128]{1,0:T(8,128)(2,1)} %q_ref.1, bf16[64,2048]{1,0:T(8,128)(2,1)} %bitcast.5, bf16[64,2048]{1,0:T(8,128)(2,1)} %bitcast.6, bf16[2048,128]{1,0:T(8,128)(2,1)} %gate_ref.1, bf16[2048,128]{1,0:T(8,128)(2,1)} %pre_ref.1, ...), custom_call_target="tpu_custom_call" | custom-call | tf_op jit(solution)/shard_map/pallas_call | solution.py:267
  26.9 2.9 %collective-permute-done.2.refs_4_ = bf16[80,2048]{1,0:T(8,128)(2,1)S(1)} collective-permute-done((bf16[80,2048]{1,0:T(8,128)(2,1)S(1)}, bf16[80,2048]{1,0:T(8,128)(2,1)S(1)}, u32[]{:S(2)}, u32[]{:S(2)}) %collective-permute-start.2) | collective-permute-done | bytes 327712 | tf_op jit(solution)/shard_map/ppermute | solution.py:258
  29.7 0.0 collective-permute-done.1.refs_3_
  29.7 0.0 copy-start.1
  29.7 0.0 copy-start.2
  29.7 4.2 %shard_map.111 = (bf16[768,640]{1,0:T(8,128)(2,1)S(1)}, bf16[144,128]{1,0:T(8,128)(2,1)S(1)}) custom-call(bf16[80,2048]{1,0:T(8,128)(2,1)S(1)} %get-tuple-element.14.refs_0_, bf16[112,2048]{1,0:T(8,128)(2,1)S(1)} %get-tuple-element.15.refs_1_, bf16[80,2048]{1,0:T(8,128)(2,1)S(1)} %collective-permute-done.refs_2_, ...), custom_call_target="tpu_custom_call" | custom-call | tf_op jit(solution)/shard_map/pallas_call | solution.py:282
  33.9 7.3 %collective-permute-start.6 = (bf16[144,128]{1,0:T(8,128)(2,1)S(1)}, bf16[144,128]{1,0:T(8,128)(2,1)S(1)}, u32[]{:S(2)}, u32[]{:S(2)}) collective-permute-start(bf16[144,128]{1,0:T(8,128)(2,1)S(1)} %get-tuple-element.21), channel_id=1, source_target_pairs={{0,4},{4,8},{8,12},{12,16},{16,20},{20,24},{24,28},{28,32},{32,36}... | collective-permute-start | bytes 110600 | tf_op jit(solution)/shard_map/ppermute | solution.py:288
  41.2 0.0 collective-permute-done.4.top_ref
  41.2 0.0 collective-permute-done.5.bottom_ref
  41.2 0.0 copy-start
  41.2 1.6 %shard_map.112 = (bf16[768,640]{1,0:T(8,128)(2,1)S(1)}, bf16[144,128]{1,0:T(8,128)(2,1)S(1)}) custom-call(bf16[768,640]{1,0:T(8,128)(2,1)S(1)} %get-tuple-element.19.near_ref, bf16[80,2048]{1,0:T(8,128)(2,1)S(1)} %collective-permute-done.4.top_ref, bf16[112,2048]{1,0:T(8,128)(2,1)S(1)} %collective-permute-done.5.bottom_ref, ...), custom_call_target="tpu_custom_call", output_to_operand_aliasing={{0}: (0, {})} | custom-call | tf_op jit(solution)/shard_map/pallas_call | solution.py:289
  42.8 7.4 %collective-permute-start.7 = (bf16[144,128]{1,0:T(8,128)(2,1)S(1)}, bf16[144,128]{1,0:T(8,128)(2,1)S(1)}, u32[]{:S(2)}, u32[]{:S(2)}) collective-permute-start(bf16[144,128]{1,0:T(8,128)(2,1)S(1)} %get-tuple-element.22), channel_id=1, source_target_pairs={{4,0},{8,4},{12,8},{16,12},{20,16},{24,20},{28,24},{32,28},{36,32}... | collective-permute-start | bytes 110600 | tf_op jit(solution)/shard_map/ppermute | solution.py:292
  50.3 0.0 copy-done.1
  50.3 0.0 copy-done.2
  50.3 2.6 %shard_map.113.refs_3_ = bf16[768,256]{1,0:T(8,128)(2,1)S(1)} custom-call(f32[2]{0:T(128)S(1)} %copy-done.2, f32[3,128]{1,0:T(4,128)S(1)} %copy-done.1, bf16[768,640]{1,0:T(8,128)(2,1)S(1)} %get-tuple-element.20.full_ref.refs_2_), custom_call_target="tpu_custom_call" | custom-call | tf_op jit(solution)/shard_map/pallas_call | solution.py:309
  52.9 0.0 collective-permute-done.6.refs_4_
  52.9 0.0 collective-permute-done.7.refs_5_
  52.9 1.6 %shard_map.114 = bf16[768,256]{1,0:T(8,128)(2,1)S(1)} custom-call(f32[2]{0:T(128)S(1)} %copy-done.2, f32[3,128]{1,0:T(4,128)S(1)} %copy-done.1, bf16[768,640]{1,0:T(8,128)(2,1)S(1)} %get-tuple-element.20.full_ref.refs_2_, bf16[768,256]{1,0:T(8,128)(2,1)S(1)} %shard_map.113.refs_3_, ...), custom_call_target="tpu_custom_call", output_to_operand_aliasing={{}: (3, {})} | custom-call | tf_op jit(solution)/shard_map/pallas_call | solution.py:310
  54.5 9.7 %all_to_all.5.parts_ref = bf16[4,192,256]{2,1,0:T(8,128)(2,1)S(1)} all-to-all(bf16[4,192,256]{2,1,0:T(8,128)(2,1)S(1)} %bitcast.4), channel_id=1, replica_groups=mesh['sp'=256,'tp'=4] {'tp'}, dimensions={0} | all-to-all | bytes 786432 | tf_op jit(solution)/shard_map/all_to_all | solution.py:311
  64.2 0.0 copy-done
  64.2 1.7 %project_out.1 = bf16[192,2048]{1,0:T(8,128)(2,1)} custom-call(bf16[4,192,256]{2,1,0:T(8,128)(2,1)S(1)} %all_to_all.5.parts_ref, bf16[1024,2048]{1,0:T(8,128)(2,1)S(1)} %copy-done), custom_call_target="tpu_custom_call" | custom-call | tf_op jit(solution)/shard_map/project_out/pallas_call | solution.py:314
Async XLA Ops:
  1.2 11.1 %collective-permute-start.3 = (bf16[112,2048]{1,0:T(8,128)(2,1)S(1)}, bf16[112,2048]{1,0:T(8,128)(2,1)S(1)}, u32[]{:S(2)}, u32[]{:S(2)}) collective-permute-start(bf16[112,2048]{1,0:T(8,128)(2,1)S(1)} %get-tuple-element.15.refs_1_), channel_id=1, source_target_pairs={{0,3},{1,2},{2,1},{3,0},{4,7},{5,6},{6,5},{7,4},{8,11},{9,10},{10,... | collective-permute-start | bytes 1376264 | tf_op jit(solution)/shard_map/ppermute | solution.py:258
  6.4 15.8 %collective-permute-start = (bf16[80,2048]{1,0:T(8,128)(2,1)S(1)}, bf16[80,2048]{1,0:T(8,128)(2,1)S(1)}, u32[]{:S(2)}, u32[]{:S(2)}) collective-permute-start(bf16[80,2048]{1,0:T(8,128)(2,1)S(1)} %get-tuple-element.14.refs_0_), channel_id=1, source_target_pairs={{0,1},{1,0},{2,3},{3,2},{4,5},{5,4},{6,7},{7,6},{8,9},{9,8},{10,11... | collective-permute-start | bytes 983048 | tf_op jit(solution)/shard_map/ppermute | solution.py:258
  8.3 21.4 %collective-permute-start.1 = (bf16[112,2048]{1,0:T(8,128)(2,1)S(1)}, bf16[112,2048]{1,0:T(8,128)(2,1)S(1)}, u32[]{:S(2)}, u32[]{:S(2)}) collective-permute-start(bf16[112,2048]{1,0:T(8,128)(2,1)S(1)} %get-tuple-element.15.refs_1_), channel_id=1, source_target_pairs={{0,1},{1,0},{2,3},{3,2},{4,5},{5,4},{6,7},{7,6},{8,9},{9,8},{10,11... | collective-permute-start | bytes 1376264 | tf_op jit(solution)/shard_map/ppermute | solution.py:258
  12.3 28.9 %collective-permute-start.5 = (bf16[112,2048]{1,0:T(8,128)(2,1)S(1)}, bf16[112,2048]{1,0:T(8,128)(2,1)S(1)}, u32[]{:S(2)}, u32[]{:S(2)}) collective-permute-start(bf16[112,2048]{1,0:T(8,128)(2,1)S(1)} %collective-permute-done.3.refs_5_), channel_id=1, source_target_pairs={{0,1},{1,0},{2,3},{3,2},{4,5},{5,4},{6,7},{7,6},{8,9},{9,8},{10,11... | collective-permute-start | bytes 1376264 | tf_op jit(solution)/shard_map/ppermute | solution.py:258
  18.4 11.3 %collective-permute-start.2 = (bf16[80,2048]{1,0:T(8,128)(2,1)S(1)}, bf16[80,2048]{1,0:T(8,128)(2,1)S(1)}, u32[]{:S(2)}, u32[]{:S(2)}) collective-permute-start(bf16[80,2048]{1,0:T(8,128)(2,1)S(1)} %get-tuple-element.14.refs_0_), channel_id=1, source_target_pairs={{0,3},{1,2},{2,1},{3,0},{4,7},{5,6},{6,5},{7,4},{8,11},{9,10},{10,... | collective-permute-start | bytes 983048 | tf_op jit(solution)/shard_map/ppermute | solution.py:258
  22.2 19.0 %collective-permute-start.4 = (bf16[80,2048]{1,0:T(8,128)(2,1)S(1)}, bf16[80,2048]{1,0:T(8,128)(2,1)S(1)}, u32[]{:S(2)}, u32[]{:S(2)}) collective-permute-start(bf16[80,2048]{1,0:T(8,128)(2,1)S(1)} %collective-permute-done.refs_2_), channel_id=1, source_target_pairs={{0,3},{1,2},{2,1},{3,0},{4,7},{5,6},{6,5},{7,4},{8,11},{9,10},{10,... | collective-permute-start | bytes 983048 | tf_op jit(solution)/shard_map/ppermute | solution.py:258
  29.7 20.5 %copy-start.1 = (f32[3,128]{1,0:T(4,128)S(1)}, f32[3,128]{1,0:T(4,128)}, u32[]{:S(2)}) copy-start(f32[3,128]{1,0:T(4,128)} %refs_1_.1) | copy-start | bytes 4612
  29.7 20.6 %copy-start.2 = (f32[2]{0:T(128)S(1)}, f32[2]{0:T(128)}, u32[]{:S(2)}) copy-start(f32[2]{0:T(128)} %refs_0_.1) | copy-start | bytes 28
  33.9 19.0 %collective-permute-start.6 = (bf16[144,128]{1,0:T(8,128)(2,1)S(1)}, bf16[144,128]{1,0:T(8,128)(2,1)S(1)}, u32[]{:S(2)}, u32[]{:S(2)}) collective-permute-start(bf16[144,128]{1,0:T(8,128)(2,1)S(1)} %get-tuple-element.21), channel_id=1, source_target_pairs={{0,4},{4,8},{8,12},{12,16},{16,20},{20,24},{24,28},{28,32},{32,36}... | collective-permute-start | bytes 110600 | tf_op jit(solution)/shard_map/ppermute | solution.py:288
  41.2 23.0 %copy-start = (bf16[1024,2048]{1,0:T(8,128)(2,1)S(1)}, bf16[1024,2048]{1,0:T(8,128)(2,1)}, u32[]{:S(2)}) copy-start(bf16[1024,2048]{1,0:T(8,128)(2,1)} %weight_ref.1) | copy-start | bytes 12582916
  42.8 10.1 %collective-permute-start.7 = (bf16[144,128]{1,0:T(8,128)(2,1)S(1)}, bf16[144,128]{1,0:T(8,128)(2,1)S(1)}, u32[]{:S(2)}, u32[]{:S(2)}) collective-permute-start(bf16[144,128]{1,0:T(8,128)(2,1)S(1)} %get-tuple-element.22), channel_id=1, source_target_pairs={{4,0},{8,4},{12,8},{16,12},{20,16},{24,20},{28,24},{32,28},{36,32}... | collective-permute-start | bytes 110600 | tf_op jit(solution)/shard_map/ppermute | solution.py:292
